TPU v7x, 32 devices: a whole 2x2x4 slice. The times are simulated.
32 devices in a mesh: fs: 8 (over z, y), tp: 4 (over x, core).
Axes of the slice: x: 2, y: 2, z: 4, core: 2. Of those that a mesh axis runs over, the one named last changes fastest.
Arguments:
- inputs: bfloat16 [4096, 2304], P('fs'), may hold values from -6 to 6
- value_cot: bfloat16 [4096, 4096], P('fs', 'tp'), may hold values from -0.09375 to 0.09375
- retained: bfloat16 [4096, 4096], P('fs', 'tp'), may hold values from -6 to 6
- output_cot: bfloat16 [4096, 2304], P('fs'), may hold values from -0.09375 to 0.09375
- proj_value: bfloat16 [2304, 192], P('fs'), may hold values from -0.125 to 0.125
- proj_output: bfloat16 [2304, 192], P('fs'), may hold values from -0.125 to 0.125
- w_value: float32 [2304, 4096], P('fs', 'tp'), may hold values from -6 to 6
- w_output: float32 [4096, 2304], P('tp', 'fs'), may hold values from -6 to 6
- first_value: float32 [192, 4096], P('fs', 'tp'), may hold values from -106 to 106
- second_value: float32 [192, 4096], P('fs', 'tp'), may hold values from 0.25 to 4
- first_output: float32 [192, 4096], P('fs', 'tp'), may hold values from -106 to 106
- second_output: float32 [192, 4096], P('fs', 'tp'), may hold values from 0.25 to 4
Outputs:
- step_value: float32 [2304, 4096], P('fs', 'tp')
- step_output: float32 [4096, 2304], P('tp', 'fs')
- copy_value: bfloat16 [2304, 4096], P(None, 'tp')
- copy_output: bfloat16 [4096, 2304], P('tp')
- new_first_value: float32 [192, 4096], P('fs', 'tp')
- new_second_value: float32 [192, 4096], P('fs', 'tp')
- new_first_output: float32 [192, 4096], P('fs', 'tp')
- new_second_output: float32 [192, 4096], P('fs', 'tp')
All inputs are finite; a program needn't handle non-finite values.
Results may differ from a plain program's by a relative error of at most 0.0034.
Values may be sent and summed in bfloat16 or wider, within the bound.
A program may use at most 64 MiB of HBM per device.

v0:
```python
import functools

import jax
import jax.numpy as jnp
from jax import lax
from jax.experimental import pallas as pl
from jax.experimental.pallas import tpu as pltpu
from jax.sharding import PartitionSpec as P

BF16 = jnp.bfloat16
F32 = jnp.float32

beta_one = 0.8
beta_two = 0.9
moment_eps = 1e-08
norm_eps = 1e-06

EARLY_NUM, EARLY_DEN = 1, 6
CHUNKS = 4


def adapt(first, second, grad):
    new_first = beta_one * first + (1.0 - beta_one) * grad
    new_second = beta_two * second + (1.0 - beta_two) * grad * grad
    direction = (new_first / (jnp.sqrt(new_second) + moment_eps)).astype(BF16)
    return (new_first, new_second, direction)


def flat(block):
    parts, rows, columns = block.shape
    if rows % 16 == 0:
        return block.reshape(parts * rows, columns)
    return block.astype(F32).reshape(parts * rows, columns).astype(block.dtype)


def exchange(
    n, t, x_ref, oc_ref, vc_ref, ret_ref, pv_ref, po_ref, wv_ref, wo_ref, fv_ref, sv_ref, fo_ref, so_ref,
    wall, pall, dall, sq, nfv, nsv, nfo, nso,
    xin, pr, gsend, grecv,
    load_sem, p_send, p_recv, core_send, core_recv, g_send, g_recv, d_send, d_recv, q_send, q_recv,
    ring_send, ring_recv, y_send, y_recv,
):
    me = lax.axis_index("fs")
    tp = lax.axis_index("tp")
    core = lax.rem(tp, 2)
    partner = tp + 1 - 2 * core
    z, y = me // 2, lax.rem(me, 2)
    levels = n // 2
    across = me + 1 - 2 * y
    q, columns = wv_ref.shape
    rows = 2 * q
    early = max(16, (rows * EARLY_NUM // EARLY_DEN) // 16 * 16)
    late = rows - early
    last = levels // 2
    halved = levels % 2 == 0
    rr = fv_ref.shape[0]

    def remote(src, dst, ssem, rsem, device):
        return pltpu.make_async_remote_copy(
            src_ref=src, dst_ref=dst, send_sem=ssem, recv_sem=rsem,
            device_id=device, device_id_type=pl.DeviceIdType.MESH,
        )

    barrier = pltpu.get_barrier_semaphore()
    for d in range(1, n):
        pl.semaphore_signal(
            barrier, inc=1, device_id={"fs": lax.rem(me + d, n)}, device_id_type=pl.DeviceIdType.MESH
        )
    for d in range(1, t):
        pl.semaphore_signal(
            barrier, inc=1, device_id={"tp": lax.rem(tp + d, t)}, device_id_type=pl.DeviceIdType.MESH
        )

    @pl.when(core == 0)
    def _():
        pltpu.make_async_copy(x_ref, xin, load_sem).start()
        pall[0, me] = pv_ref[...]

    @pl.when(core == 1)
    def _():
        pltpu.make_async_copy(oc_ref, xin, load_sem).start()
        pall[1, me] = po_ref[...]

    wall[me, :q] = wv_ref[...].astype(BF16)
    wall[me, q:] = wo_ref[...].astype(BF16)
    pl.semaphore_wait(barrier, n - 1 + t - 1)

    sends = []

    def go(copy):
        copy.start()
        sends.append(copy)
        return copy

    def to_all(buffer, target, ssem, rsem):
        out = []
        for d in range(1, n):
            peer = lax.rem(me + d, n)
            out.append(go(remote(buffer(peer), target, ssem.at[d], rsem.at[d], {"fs": peer})))
        return out

    def spread(place, ssem, rsem):
        own = place(me)
        first = [go(remote(own, own, ssem.at[0], rsem.at[0], {"fs": across}))]
        for d in range(1, levels):
            target = lax.rem(z + d, levels) * 2 + y
            first.append(go(remote(own, own, ssem.at[d], rsem.at[d], {"fs": target})))
        return first

    def pass_on(first, place, ssem, rsem):
        second = []
        for d in range(1, levels):
            first[d].wait_recv()
            block = place(lax.rem(z + levels - d, levels) * 2 + y)
            second.append(
                go(remote(block, block, ssem.at[levels + d], rsem.at[levels + d], {"fs": across}))
            )
        return first[:1] + second

    def edge(piece):
        return late if piece == CHUNKS else late * piece // CHUNKS // 16 * 16

    def span(piece, k, s):
        low, high = (edge(piece), edge(piece + 1)) if piece < CHUNKS else (late, rows)
        if halved and k == last:
            middle = low + (high - low) // 2 // 16 * 16
            low, high = (low, middle) if s == 0 else (middle, high)
        return low, high - low

    def at(level, column, low, size):
        return wall.at[level * 2 + column, pl.ds(low, size)]

    def ring(piece, k, s):
        low, size = span(piece, k, s)
        if size == 0:
            return None
        step = 1 if s == 0 else levels - 1
        level = lax.rem(z + (levels - step) * (k - 1), levels)
        column = y if piece <= CHUNKS else 1 - y
        place = at(level, column, low, size)
        target = lax.rem(z + step, levels) * 2 + y
        return go(remote(place, place, ring_send.at[s, k, piece], ring_recv.at[s, k, piece], {"fs": target}))

    def over(piece, k, s):
        low, size = span(piece, k, s)
        if size == 0:
            return None
        step = 1 if s == 0 else levels - 1
        level = lax.rem(z + (levels - step) * k, levels)
        place = at(level, y, low, size)
        return go(remote(place, place, y_send.at[s, k, piece], y_recv.at[s, k, piece], {"fs": across}))

    def landed(copy):
        if copy is not None:
            copy.wait_recv()

    proj_first = spread(lambda block: pall.at[core, block], p_send, p_recv)
    own_early = at(z, y, late, early)
    crossed = go(remote(own_early, own_early, y_send.at[1, 0, 0], y_recv.at[1, 0, 0], {"fs": across}))
    steps = {}
    for piece in range(CHUNKS + 1):
        for s in (0, 1):
            steps[piece, 1, s] = ring(piece, 1, s)
    proj_copies = pass_on(proj_first, lambda block: pall.at[core, block], p_send, p_recv)
    overs = [over(piece, 0, 0) for piece in range(CHUNKS)]

    for copy in proj_copies:
        copy.wait_recv()
    whole_proj = go(remote(pall.at[core], pall.at[core], core_send.at[0], core_recv.at[0], {"tp": partner}))
    pltpu.make_async_copy(x_ref, xin, load_sem).wait()
    pr[core] = jnp.dot(xin[...], flat(pall[core]), preferred_element_type=F32).astype(BF16)
    swapped = go(remote(pr.at[core], pr.at[core], core_send.at[1], core_recv.at[1], {"tp": partner}))
    swapped.wait_recv()
    for side, cot in ((0, vc_ref), (1, ret_ref)):
        grad = lax.dot_general(
            pr[side], cot[...], (((0,), (0,)), ((), ())), preferred_element_type=F32
        )
        for peer in range(n):
            gsend[peer, :, side * columns:(side + 1) * columns] = (
                grad[peer * rr:(peer + 1) * rr].astype(BF16)
            )
    grad_copies = to_all(lambda peer: gsend.at[peer], grecv.at[me], g_send, g_recv)

    crossed.wait_recv()
    for s in (0, 1):
        steps[CHUNKS + 1, 1, s] = ring(CHUNKS + 1, 1, s)

    for k in range(1, last + 1):
        for piece in range(CHUNKS + 2):
            if k == 1 and piece == CHUNKS + 1:
                for copy in grad_copies:
                    copy.wait_recv()
                total = gsend[me].astype(F32)
                for d in range(1, n):
                    total += grecv[lax.rem(me + d, n)].astype(F32)
                for side, refs in ((0, (fv_ref, sv_ref, nfv, nsv)), (1, (fo_ref, so_ref, nfo, nso))):
                    part = total[:, side * columns:(side + 1) * columns]
                    new_first, new_second, direction = adapt(refs[0][...], refs[1][...], part)
                    refs[2][...] = new_first
                    refs[3][...] = new_second
                    dall[me, :, side * columns:(side + 1) * columns] = direction
                dir_first = spread(lambda block: dall.at[block], d_send, d_recv)
            for s in (0, 1):
                landed(steps[piece, k, s])
                if k < last:
                    steps[piece, k + 1, s] = ring(piece, k + 1, s)
                if piece < CHUNKS:
                    overs.append(over(piece, k, s))

    for copy in pass_on(dir_first, lambda block: dall.at[block], d_send, d_recv):
        copy.wait_recv()
    sums = []
    for side in (0, 1):
        acc = jnp.zeros((rr, columns), F32)
        for k in range(n):
            acc += jnp.square(dall[k, :, side * columns:(side + 1) * columns].astype(F32))
        sums.append(jnp.sum(acc))
    line = lax.broadcasted_iota(jnp.int32, sq.shape[1:], 0)
    sq[tp] = jnp.where(line == 0, sums[0], sums[1])
    sq_copies = []
    for d in range(1, t):
        sq_copies.append(
            go(remote(sq.at[tp], sq.at[tp], q_send.at[d], q_recv.at[d], {"tp": lax.rem(tp + d, t)}))
        )
    for copy in sq_copies:
        copy.wait_recv()
    for copy in overs:
        landed(copy)
    whole_proj.wait_recv()
    for copy in sends:
        copy.wait_send()


def finish(q, count, sq_ref, wall_ref, pall_ref, own_v, own_o, dv_ref, do_ref, step_v, step_o, copy_v, copy_o):
    totals = jnp.sum(sq_ref[...], axis=0)
    scale_v = lax.rsqrt(totals[0:1, 0:1] / count + norm_eps)
    scale_o = lax.rsqrt(totals[1:2, 0:1] / count + norm_eps)
    n, _, lanes = wall_ref.shape
    dir_v, dir_o = dv_ref[...], do_ref[...]
    step_v[...] = jnp.dot(own_v[...], dir_v, preferred_element_type=F32) * scale_v
    step_o[...] = jnp.dot(own_o[...], dir_o, preferred_element_type=F32) * scale_o
    w_v = wall_ref[:, :q].astype(F32).reshape(n * q, lanes)
    w_o = wall_ref[:, q:].astype(F32).reshape(n * q, lanes)
    copy_v[...] = (
        w_v + jnp.dot(pall_ref[0], dir_v, preferred_element_type=F32) * scale_v
    ).astype(BF16)
    moved = w_o + jnp.dot(pall_ref[1], dir_o, preferred_element_type=F32) * scale_o
    copy_o[...] = moved.T.astype(BF16)


def per_device(
    n, t,
    inputs, value_cot, retained, output_cot, proj_value, proj_output, w_value, w_output,
    first_value, second_value, first_output, second_output,
):
    tokens, width = inputs.shape
    q, rank = proj_value.shape
    columns = value_cot.shape[1]
    rr = first_value.shape[0]
    last = n // 2 // 2
    vmem = pl.BlockSpec(memory_space=pltpu.VMEM)
    anywhere = pl.BlockSpec(memory_space=pl.ANY)
    dma = pltpu.SemaphoreType.DMA
    moment = jax.ShapeDtypeStruct((rr, columns), F32)
    wall, pall, dall, sq, first_v, second_v, first_o, second_o = pl.pallas_call(
        functools.partial(exchange, n, t),
        out_shape=(
            jax.ShapeDtypeStruct((n, 2 * q, columns), BF16),
            jax.ShapeDtypeStruct((2, n, q, rank), BF16),
            jax.ShapeDtypeStruct((n, rr, 2 * columns), BF16),
            jax.ShapeDtypeStruct((t, 8, 128), F32),
            moment, moment, moment, moment,
        ),
        in_specs=[anywhere, anywhere] + [vmem] * 10,
        out_specs=(vmem,) * 8,
        scratch_shapes=[
            pltpu.VMEM((tokens, width), BF16),
            pltpu.VMEM((2, tokens, rank), BF16),
            pltpu.VMEM((n, rr, 2 * columns), BF16),
            pltpu.VMEM((n, rr, 2 * columns), BF16),
            dma, dma((n,)), dma((n,)), dma((2,)), dma((2,)), dma((n,)), dma((n,)), dma((n,)), dma((n,)),
            dma((t,)), dma((t,)),
            dma((2, last + 1, CHUNKS + 2)), dma((2, last + 1, CHUNKS + 2)),
            dma((2, last + 1, CHUNKS)), dma((2, last + 1, CHUNKS)),
        ],
        compiler_params=pltpu.CompilerParams(
            collective_id=0, has_side_effects=True, vmem_limit_bytes=60 * 1024 * 1024
        ),
        name="exchange",
    )(
        inputs, output_cot, value_cot, retained, proj_value, proj_output, w_value, w_output.T,
        first_value, second_value, first_output, second_output,
    )
    lanes = 128
    tiles = columns // lanes
    dirs = dall.reshape(n * rr, 2 * columns)
    full = n * q
    step_v, step_o, copy_v, copy_o = pl.pallas_call(
        functools.partial(finish, q, float(rank * columns * t)),
        grid=(tiles,),
        out_shape=(
            jax.ShapeDtypeStruct((q, columns), F32),
            jax.ShapeDtypeStruct((q, columns), F32),
            jax.ShapeDtypeStruct((full, columns), BF16),
            jax.ShapeDtypeStruct((columns, full), BF16),
        ),
        in_specs=[
            pl.BlockSpec((t, 8, 128), lambda j: (0, 0, 0)),
            pl.BlockSpec((n, 2 * q, lanes), lambda j: (0, 0, j)),
            pl.BlockSpec((2, full, rank), lambda j: (0, 0, 0)),
            pl.BlockSpec((q, rank), lambda j: (0, 0)),
            pl.BlockSpec((q, rank), lambda j: (0, 0)),
            pl.BlockSpec((rank, lanes), lambda j: (0, j)),
            pl.BlockSpec((rank, lanes), lambda j: (0, j + tiles)),
        ],
        out_specs=(
            pl.BlockSpec((q, lanes), lambda j: (0, j)),
            pl.BlockSpec((q, lanes), lambda j: (0, j)),
            pl.BlockSpec((full, lanes), lambda j: (0, j)),
            pl.BlockSpec((lanes, full), lambda j: (j, 0)),
        ),
        compiler_params=pltpu.CompilerParams(vmem_limit_bytes=48 * 1024 * 1024),
        name="finish",
    )(sq, wall, pall.reshape(2, full, rank), proj_value, proj_output, dirs, dirs)
    return (step_v, step_o.T, copy_v, copy_o, first_v, second_v, first_o, second_o)


def solution(mesh):
    in_specs = (
        P("fs", None),
        P("fs", "tp"),
        P("fs", "tp"),
        P("fs", None),
        P("fs", None),
        P("fs", None),
        P("fs", "tp"),
        P("tp", "fs"),
        P("fs", "tp"),
        P("fs", "tp"),
        P("fs", "tp"),
        P("fs", "tp"),
    )
    out_specs = (
        P("fs", "tp"),
        P("tp", "fs"),
        P(None, "tp"),
        P("tp", None),
        P("fs", "tp"),
        P("fs", "tp"),
        P("fs", "tp"),
        P("fs", "tp"),
    )
    return jax.shard_map(
        functools.partial(per_device, mesh.shape["fs"], mesh.shape["tp"]),
        mesh=mesh, in_specs=in_specs, out_specs=out_specs, check_vma=False,
    )
```

profile of v0, /device:TPU:13, one launch (start us, length us, event | category | flops | bytes accessed | tf_op | source)
XLA Modules:
  0.0 170.2 jit_solution(3161248524397637789)
XLA Ops:
  0.6 0.0 copy-start.2
  0.6 0.0 copy-start.3
  0.7 151.2 %exchange.1 = (bf16[8,576,1024]{2,1,0:T(8,128)(2,1)}, bf16[2,8,288,192]{3,2,1,0:T(8,128)(2,1)}, bf16[8,24,2048]{2,1,0:T(8,128)(2,1)}, f32[4,8,128]{2,1,0:T(8,128...) custom-call(bf16[512,2304]{1,0:T(8,128)(2,1)} %x_ref.1, ...), custom_call_target="tpu_custom_call" | custom-call | tf_op jit(solution)/shard_map/exchange/pallas_call | solution.py:265
  151.9 0.0 copy-done.2
  151.9 0.0 copy-done.3
  151.9 0.0 copy-start
  151.9 1.1 copy-done
  153.1 0.0 copy-start.1
  153.1 1.7 copy-done.1
  154.7 0.0 copy-start.4
  154.7 0.7 copy-done.4
  155.4 0.0 copy-start.8
  155.4 0.0 copy-start.7
  155.4 0.0 copy-start.6
  155.5 0.0 copy-start.5
  155.5 12.2 %finish.1 = (f32[288,1024]{1,0:T(8,128)}, f32[288,1024]{1,0:T(8,128)}, bf16[2304,1024]{1,0:T(8,128)(2,1)}, bf16[1024,2304]{1,0:T(8,128)(2,1)}) custom-call(f32[4,8,128]{2,1,0:T(8,128)S(1)} %copy-done.4, bf16[8,576,1024]{2,1,0:T(8,128)(2,1)} %get-tuple-element.21.wall_ref, bf16[2,2304,192]{2,1,0:T(8,128)(2,1)S(1)} %bitcast.6, bf16[288,192]{1,0:T(8,128)(2,1)S(1)} %copy-done.2, ...), custom_call_target="tpu_custom_call" | custom-call | tf_op jit(solution)/shard_map/finish/pallas_call | solution.py:298
  167.6 0.0 copy-done.8
  167.6 0.6 copy.24
  168.3 0.0 copy-done.7
  168.3 0.6 copy.25
  168.9 0.0 copy-done.6
  168.9 0.6 copy.26
  169.6 0.0 copy-done.5
  169.6 0.6 copy.27
Async XLA Ops:
  0.6 151.3 %copy-start.2 = (bf16[288,192]{1,0:T(8,128)(2,1)S(1)}, bf16[288,192]{1,0:T(8,128)(2,1)}, u32[]{:S(2)}) copy-start(bf16[288,192]{1,0:T(8,128)(2,1)} %own_v.1) | copy-start | bytes 331780
  0.6 151.3 %copy-start.3 = (bf16[288,192]{1,0:T(8,128)(2,1)S(1)}, bf16[288,192]{1,0:T(8,128)(2,1)}, u32[]{:S(2)}) copy-start(bf16[288,192]{1,0:T(8,128)(2,1)} %own_o.1) | copy-start | bytes 331780
  151.9 1.1 copy-start
  153.1 1.7 copy-start.1
  154.7 0.7 copy-start.4
  155.4 12.2 %copy-start.8 = (f32[24,1024]{1,0:T(8,128)S(1)}, f32[24,1024]{1,0:T(8,128)}, u32[]{:S(2)}) copy-start(f32[24,1024]{1,0:T(8,128)} %get-tuple-element.44) | copy-start | bytes 294916
  155.4 12.8 %copy-start.7 = (f32[24,1024]{1,0:T(8,128)S(1)}, f32[24,1024]{1,0:T(8,128)}, u32[]{:S(2)}) copy-start(f32[24,1024]{1,0:T(8,128)} %get-tuple-element.45) | copy-start | bytes 294916
  155.4 13.5 %copy-start.6 = (f32[24,1024]{1,0:T(8,128)S(1)}, f32[24,1024]{1,0:T(8,128)}, u32[]{:S(2)}) copy-start(f32[24,1024]{1,0:T(8,128)} %get-tuple-element.46) | copy-start | bytes 294916
  155.5 14.1 %copy-start.5 = (f32[24,1024]{1,0:T(8,128)S(1)}, f32[24,1024]{1,0:T(8,128)}, u32[]{:S(2)}) copy-start(f32[24,1024]{1,0:T(8,128)} %get-tuple-element.47) | copy-start | bytes 294916
where the time goes:
time: 171 us; the launch traced here: 170 us
  Pallas kernels  163 us (95%)
  local copies, waits for them, and re-layouts  6.09 us (4%)
    pallas_call x1, Pallas kernels, per_device(): pl.pallas_call(functools.partial(exchange, n, t), out_shape=(jax.ShapeDty...  151 us
    pallas_call x1, Pallas kernels, per_device(): pl.pallas_call(functools.partial(finish, q, float(rank * columns * t)), g...  12.2 us
    unnamed x22, local copies, waits for them, and re-layouts  6.09 us

commit v1 on v0

v1 whole, which is shorter than its diff:
```python
import functools

import jax
import jax.numpy as jnp
from jax import lax
from jax.experimental import pallas as pl
from jax.experimental.pallas import tpu as pltpu
from jax.sharding import PartitionSpec as P

BF16 = jnp.bfloat16
F32 = jnp.float32

beta_one = 0.8
beta_two = 0.9
moment_eps = 1e-08
norm_eps = 1e-06

PIECES = 12
EARLY = 2
DEPTH = 3
HOOKS = (3, 5, 6, 12, 17, 22, 27)


def adapt(first, second, grad):
    new_first = beta_one * first + (1.0 - beta_one) * grad
    new_second = beta_two * second + (1.0 - beta_two) * grad * grad
    direction = (new_first / (jnp.sqrt(new_second) + moment_eps)).astype(BF16)
    return (new_first, new_second, direction)


def flat(block):
    parts, rows, columns = block.shape
    if rows % 16 == 0:
        return block.reshape(parts * rows, columns)
    return block.astype(F32).reshape(parts * rows, columns).astype(block.dtype)


def cut(rows):
    if rows % (16 * PIECES) == 0:
        return PIECES, EARLY
    count = rows // 16
    return count, max(1, count * EARLY // PIECES)


def share(q, t):
    ways = t // 2
    return ways if q % (16 * ways) == 0 else 1


def schedule(levels, count, early):
    line, sent = [], {}
    for s in range(levels - 1):
        for i in range(count):
            sent[s + 1, i] = len(line)
            line.append((0, s, i))
        for i in range(count - early, count):
            line.append((1, s, i))
    over = {}
    slot = 0
    for i in list(range(count - early, count)) + list(range(count - early)):
        over[slot] = (0, i)
        slot += 1
    for j in range(1, levels):
        for i in range(count - early):
            slot = max(slot, sent[j, i] + 3)
            over[slot] = (j, i)
            slot += 1
    return line, over, max(len(line), slot)


def exchange(
    n, t, x_ref, oc_ref, vc_ref, ret_ref, pv_ref, po_ref, wv_ref, wo_ref, fv_ref, sv_ref, fo_ref, so_ref,
    wall, pall, dall, sq, nfv, nsv, nfo, nso,
    xin, pr, gsend, gacross, gpart, grecv,
    load_sem, p_send, p_recv, x_send, x_recv, core_send, core_recv, ga_send, ga_recv, g_send, g_recv,
    d_send, d_recv, q_send, q_recv, up_send, down_send, over_send, w_recv,
):
    me = lax.axis_index("fs")
    tp = lax.axis_index("tp")
    core = lax.rem(tp, 2)
    partner = tp + 1 - 2 * core
    x = tp // 2
    z, y = me // 2, lax.rem(me, 2)
    levels = n // 2
    across = me + 1 - 2 * y
    q, columns = wv_ref.shape
    rows = 2 * q
    rr = fv_ref.shape[0]
    count, early = cut(rows)
    size = rows // count
    ways = share(q, t)
    part_rows = q // ways

    def remote(src, dst, ssem, rsem, device):
        return pltpu.make_async_remote_copy(
            src_ref=src, dst_ref=dst, send_sem=ssem, recv_sem=rsem,
            device_id=device, device_id_type=pl.DeviceIdType.MESH,
        )

    barrier = pltpu.get_barrier_semaphore()
    for d in range(1, n):
        pl.semaphore_signal(
            barrier, inc=1, device_id={"fs": lax.rem(me + d, n)}, device_id_type=pl.DeviceIdType.MESH
        )
    for d in range(1, t):
        pl.semaphore_signal(
            barrier, inc=1, device_id={"tp": lax.rem(tp + d, t)}, device_id_type=pl.DeviceIdType.MESH
        )

    @pl.when(core == 0)
    def _():
        pltpu.make_async_copy(x_ref, xin, load_sem).start()
        pall[0, me] = pv_ref[...]

    @pl.when(core == 1)
    def _():
        pltpu.make_async_copy(oc_ref, xin, load_sem).start()
        pall[1, me] = po_ref[...]

    wall[me, :q] = wv_ref[...].astype(BF16)
    wall[me, q:] = wo_ref[...].astype(BF16)
    pl.semaphore_wait(barrier, n - 1 + t - 1)

    sends = []

    def go(copy):
        copy.start()
        sends.append(copy)
        return copy

    def spread(place, ssem, rsem):
        own = place(me)
        first = [go(remote(own, own, ssem.at[0], rsem.at[0], {"fs": across}))]
        for d in range(1, levels):
            target = lax.rem(z + d, levels) * 2 + y
            first.append(go(remote(own, own, ssem.at[d], rsem.at[d], {"fs": target})))
        return first

    def pass_on(first, place, ssem, rsem):
        second = []
        for d in range(1, levels):
            first[d].wait_recv()
            block = place(lax.rem(z + levels - d, levels) * 2 + y)
            second.append(
                go(remote(block, block, ssem.at[levels + d], rsem.at[levels + d], {"fs": across}))
            )
        return first[:1] + second

    line, over, slots = schedule(levels, count, early)

    def piece(level, side, i):
        column = y if side == 0 else 1 - y
        return wall.at[level * 2 + column, pl.ds(i * size, size)]

    def along(slot, step):
        side, s, i = line[slot]
        place = piece(z - s if step > 0 else z + s, side, i)
        ssem = (up_send if step > 0 else down_send).at[slot % DEPTH]
        level = z - s if step > 0 else z + s
        return remote(place, place, ssem, w_recv.at[side, level, i], {"fs": (z + step) * 2 + y})

    def goes(slot, step):
        s = line[slot][1]
        if step > 0:
            return jnp.logical_and(z >= s, z < levels - 1)
        return jnp.logical_and(z + s < levels, z > 0)

    def nearest(j):
        if j == 0:
            return z
        low = jnp.minimum(z, levels - 1 - z)
        near = z + (j + 1) // 2 * (1 if j % 2 else -1)
        far = jnp.where(z < levels - 1 - z, j, levels - 1 - j)
        return jnp.where(j <= 2 * low, near, far)

    def crossing(slot):
        j, i = over[slot]
        level = nearest(j)
        place = piece(level, 0, i)
        return remote(place, place, over_send.at[slot % DEPTH], w_recv.at[1, level, i], {"fs": across})

    held = set()

    def landed(side, level, i):
        place = piece(level, side, i)
        remote(place, place, over_send.at[0], w_recv.at[side, level, i], {"fs": across}).wait_recv()

    def ensure(side, k, i):
        if (side, k, i) in held:
            return
        held.add((side, k, i))
        if k == 0:
            landed(side, z, i)
            return

        @pl.when(z >= k)
        def _():
            landed(side, z - k, i)

        @pl.when(z + k < levels)
        def _():
            landed(side, z + k, i)

    def drained(slot):
        if 0 <= slot < len(line):
            for step in (1, -1):
                @pl.when(goes(slot, step))
                def _():
                    along(slot, step).wait_send()
        if slot in over:
            crossing(slot).wait_send()

    def advance(slot):
        drained(slot - DEPTH)
        if slot < len(line):
            side, s, i = line[slot]
            if side == 1 or s > 0:
                ensure(side, s, i)
            for step in (1, -1):
                @pl.when(goes(slot, step))
                def _():
                    along(slot, step).start()
        if slot in over:
            j, i = over[slot]
            for k in range(1, j + 1):
                ensure(0, k, i)
            crossing(slot).start()

    chain = {}

    def part(block):
        return pall.at[core, block, pl.ds(x * part_rows, part_rows)]

    def shared(block):
        for d in range(1, ways):
            place = part(block)
            target = lax.rem(x + d, ways) * 2 + core
            chain["shared"].append(
                go(remote(place, place, x_send.at[d, block], x_recv.at[d, block], {"tp": target}))
            )

    def hook_pass():
        first = chain["proj"]
        second = pass_on(first, part, p_send, p_recv)
        for d in range(1, levels):
            shared(lax.rem(z + levels - d, levels) * 2 + y)
        chain["proj"] = second

    def hook_share():
        second = chain["proj"]
        for d, copy in enumerate(second):
            copy.wait_recv()
            shared(lax.rem(z + levels - d, levels) * 2 + 1 - y)

    def hook_grads():
        for copy in chain["shared"]:
            copy.wait_recv()
        chain["whole"] = go(
            remote(pall.at[core], pall.at[core], core_send.at[0], core_recv.at[0], {"tp": partner})
        )
        pltpu.make_async_copy(x_ref, xin, load_sem).wait()
        pr[core] = jnp.dot(xin[...], flat(pall[core]), preferred_element_type=F32).astype(BF16)
        swapped = go(remote(pr.at[core], pr.at[core], core_send.at[1], core_recv.at[1], {"tp": partner}))
        swapped.wait_recv()
        for side, cot in ((0, vc_ref), (1, ret_ref)):
            grad = lax.dot_general(
                pr[side], cot[...], (((0,), (0,)), ((), ())), preferred_element_type=F32
            )
            for peer in range(n):
                gsend[peer % 2, peer // 2, :, side * columns:(side + 1) * columns] = (
                    grad[peer * rr:(peer + 1) * rr].astype(BF16)
                )
        chain["ga"] = go(
            remote(gsend.at[1 - y], gacross, ga_send.at[0], ga_recv.at[0], {"fs": across})
        )

    def hook_partial():
        chain["ga"].wait_recv()
        gpart[...] = (gsend[y].astype(F32) + gacross[...].astype(F32)).astype(BF16)
        copies = []
        for d in range(1, levels):
            level = lax.rem(z + d, levels)
            copies.append(
                go(remote(gpart.at[level], grecv.at[z], g_send.at[d], g_recv.at[d], {"fs": level * 2 + y}))
            )
        chain["g"] = copies

    def hook_moments():
        for copy in chain["g"]:
            copy.wait_recv()
        total = gsend[y, z].astype(F32) + gacross[z].astype(F32)
        for d in range(1, levels):
            total += grecv[lax.rem(z + levels - d, levels)].astype(F32)
        for side, refs in ((0, (fv_ref, sv_ref, nfv, nsv)), (1, (fo_ref, so_ref, nfo, nso))):
            grad = total[:, side * columns:(side + 1) * columns]
            new_first, new_second, direction = adapt(refs[0][...], refs[1][...], grad)
            refs[2][...] = new_first
            refs[3][...] = new_second
            dall[me, :, side * columns:(side + 1) * columns] = direction
        chain["dirs"] = spread(lambda block: dall.at[block], d_send, d_recv)

    def hook_dirs():
        chain["dirs"] = pass_on(chain["dirs"], lambda block: dall.at[block], d_send, d_recv)

    def hook_sums():
        for copy in chain["dirs"]:
            copy.wait_recv()
        sums = []
        for side in (0, 1):
            acc = jnp.zeros((rr, columns), F32)
            for k in range(n):
                acc += jnp.square(dall[k, :, side * columns:(side + 1) * columns].astype(F32))
            sums.append(jnp.sum(acc))
        row = lax.broadcasted_iota(jnp.int32, sq.shape[1:], 0)
        sq[tp] = jnp.where(row == 0, sums[0], sums[1])
        chain["sq"] = [
            go(remote(sq.at[tp], sq.at[tp], q_send.at[d], q_recv.at[d], {"tp": lax.rem(tp + d, t)}))
            for d in range(1, t)
        ]

    hooks = dict(zip(
        HOOKS, (hook_pass, hook_share, hook_grads, hook_partial, hook_moments, hook_dirs, hook_sums)
    ))
    chain["shared"] = []
    chain["proj"] = spread(part, p_send, p_recv)
    end = max(slots, max(HOOKS) + 1)
    for slot in range(end):
        if slot in hooks:
            hooks[slot]()
        advance(slot)
    for slot in range(end, slots + DEPTH):
        drained(slot - DEPTH)

    for k in range(1, levels):
        for i in range(count):
            ensure(0, k, i)
        for i in range(count - early, count):
            ensure(1, k, i)
    for j in range(levels):
        for i in range(count - early):
            landed(1, nearest(j), i)
    for copy in chain["sq"]:
        copy.wait_recv()
    chain["whole"].wait_recv()
    for copy in sends:
        copy.wait_send()


def finish(q, count, sq_ref, wall_ref, pall_ref, own_v, own_o, dv_ref, do_ref, step_v, step_o, copy_v, copy_o):
    totals = jnp.sum(sq_ref[...], axis=0)
    scale_v = lax.rsqrt(totals[0:1, 0:1] / count + norm_eps)
    scale_o = lax.rsqrt(totals[1:2, 0:1] / count + norm_eps)
    n, _, lanes = wall_ref.shape
    dir_v, dir_o = dv_ref[...], do_ref[...]
    step_v[...] = jnp.dot(own_v[...], dir_v, preferred_element_type=F32) * scale_v
    step_o[...] = jnp.dot(own_o[...], dir_o, preferred_element_type=F32) * scale_o
    w_v = wall_ref[:, :q].astype(F32).reshape(n * q, lanes)
    w_o = wall_ref[:, q:].astype(F32).reshape(n * q, lanes)
    copy_v[...] = (
        w_v + jnp.dot(pall_ref[0], dir_v, preferred_element_type=F32) * scale_v
    ).astype(BF16)
    moved = w_o + jnp.dot(pall_ref[1], dir_o, preferred_element_type=F32) * scale_o
    copy_o[...] = moved.T.astype(BF16)


def per_device(
    n, t,
    inputs, value_cot, retained, output_cot, proj_value, proj_output, w_value, w_output,
    first_value, second_value, first_output, second_output,
):
    tokens, width = inputs.shape
    q, rank = proj_value.shape
    columns = value_cot.shape[1]
    rr = first_value.shape[0]
    levels = n // 2
    pieces, _ = cut(2 * q)
    ways = share(q, t)
    vmem = pl.BlockSpec(memory_space=pltpu.VMEM)
    anywhere = pl.BlockSpec(memory_space=pl.ANY)
    dma = pltpu.SemaphoreType.DMA
    moment = jax.ShapeDtypeStruct((rr, columns), F32)
    wall, pall, dall, sq, first_v, second_v, first_o, second_o = pl.pallas_call(
        functools.partial(exchange, n, t),
        out_shape=(
            jax.ShapeDtypeStruct((n, 2 * q, columns), BF16),
            jax.ShapeDtypeStruct((2, n, q, rank), BF16),
            jax.ShapeDtypeStruct((n, rr, 2 * columns), BF16),
            jax.ShapeDtypeStruct((t, 8, 128), F32),
            moment, moment, moment, moment,
        ),
        in_specs=[anywhere, anywhere] + [vmem] * 10,
        out_specs=(vmem,) * 8,
        scratch_shapes=[
            pltpu.VMEM((tokens, width), BF16),
            pltpu.VMEM((2, tokens, rank), BF16),
            pltpu.VMEM((2, levels, rr, 2 * columns), BF16),
            pltpu.VMEM((levels, rr, 2 * columns), BF16),
            pltpu.VMEM((levels, rr, 2 * columns), BF16),
            pltpu.VMEM((levels, rr, 2 * columns), BF16),
            dma, dma((n,)), dma((n,)), dma((ways, n)), dma((ways, n)), dma((2,)), dma((2,)),
            dma((1,)), dma((1,)), dma((levels,)), dma((levels,)), dma((n,)), dma((n,)),
            dma((t,)), dma((t,)),
            dma((DEPTH,)), dma((DEPTH,)), dma((DEPTH,)), dma((2, levels, pieces)),
        ],
        compiler_params=pltpu.CompilerParams(
            collective_id=0, has_side_effects=True, vmem_limit_bytes=60 * 1024 * 1024
        ),
        name="exchange",
    )(
        inputs, output_cot, value_cot, retained, proj_value, proj_output, w_value, w_output.T,
        first_value, second_value, first_output, second_output,
    )
    lanes = 128
    tiles = columns // lanes
    dirs = dall.reshape(n * rr, 2 * columns)
    full = n * q
    step_v, step_o, copy_v, copy_o = pl.pallas_call(
        functools.partial(finish, q, float(rank * columns * t)),
        grid=(tiles,),
        out_shape=(
            jax.ShapeDtypeStruct((q, columns), F32),
            jax.ShapeDtypeStruct((q, columns), F32),
            jax.ShapeDtypeStruct((full, columns), BF16),
            jax.ShapeDtypeStruct((columns, full), BF16),
        ),
        in_specs=[
            pl.BlockSpec((t, 8, 128), lambda j: (0, 0, 0)),
            pl.BlockSpec((n, 2 * q, lanes), lambda j: (0, 0, j)),
            pl.BlockSpec((2, full, rank), lambda j: (0, 0, 0)),
            pl.BlockSpec((q, rank), lambda j: (0, 0)),
            pl.BlockSpec((q, rank), lambda j: (0, 0)),
            pl.BlockSpec((rank, lanes), lambda j: (0, j)),
            pl.BlockSpec((rank, lanes), lambda j: (0, j + tiles)),
        ],
        out_specs=(
            pl.BlockSpec((q, lanes), lambda j: (0, j)),
            pl.BlockSpec((q, lanes), lambda j: (0, j)),
            pl.BlockSpec((full, lanes), lambda j: (0, j)),
            pl.BlockSpec((lanes, full), lambda j: (j, 0)),
        ),
        compiler_params=pltpu.CompilerParams(vmem_limit_bytes=48 * 1024 * 1024),
        name="finish",
    )(sq, wall, pall.reshape(2, full, rank), proj_value, proj_output, dirs, dirs)
    return (step_v, step_o.T, copy_v, copy_o, first_v, second_v, first_o, second_o)


def solution(mesh):
    in_specs = (
        P("fs", None),
        P("fs", "tp"),
        P("fs", "tp"),
        P("fs", None),
        P("fs", None),
        P("fs", None),
        P("fs", "tp"),
        P("tp", "fs"),
        P("fs", "tp"),
        P("fs", "tp"),
        P("fs", "tp"),
        P("fs", "tp"),
    )
    out_specs = (
        P("fs", "tp"),
        P("tp", "fs"),
        P(None, "tp"),
        P("tp", None),
        P("fs", "tp"),
        P("fs", "tp"),
        P("fs", "tp"),
        P("fs", "tp"),
    )
    return jax.shard_map(
        functools.partial(per_device, mesh.shape["fs"], mesh.shape["tp"]),
        mesh=mesh, in_specs=in_specs, out_specs=out_specs, check_vma=False,
    )
```

time: 171 us -> 158 us (0.924)
  Pallas kernels: 163 us -> 151 us
    pallas_call x1, Pallas kernels: 151 us -> 139 us  [per_device(): pl.pallas_call(functools.partial(exchange, n, t), out_shape=(jax.ShapeDty...]
where the time goes in v1:
time: 158 us
  Pallas kernels  151 us (96%)
  local copies, waits for them, and re-layouts  6.09 us (4%)
    pallas_call x1, Pallas kernels, per_device(): pl.pallas_call(functools.partial(exchange, n, t), out_shape=(jax.ShapeDty...  139 us
    pallas_call x1, Pallas kernels, per_device(): pl.pallas_call(functools.partial(finish, q, float(rank * columns * t)), g...  12.2 us
    unnamed x22, local copies, waits for them, and re-layouts  6.09 us

profile of v1, /device:TPU:13, one launch (start us, length us, event | category | flops | bytes accessed | tf_op | source)
XLA Modules:
  0.0 157.5 jit_solution(8009575493538913778)
XLA Ops:
  0.6 0.0 copy-start.2
  0.6 0.0 copy-start.3
  0.7 138.6 %exchange.1 = (bf16[8,576,1024]{2,1,0:T(8,128)(2,1)}, bf16[2,8,288,192]{3,2,1,0:T(8,128)(2,1)}, bf16[8,24,2048]{2,1,0:T(8,128)(2,1)}, f32[4,8,128]{2,1,0:T(8,128...) custom-call(bf16[512,2304]{1,0:T(8,128)(2,1)} %x_ref.1, ...), custom_call_target="tpu_custom_call" | custom-call | tf_op jit(solution)/shard_map/exchange/pallas_call | solution.py:382
  139.3 0.0 copy-done.2
  139.3 0.0 copy-done.3
  139.3 0.0 copy-start
  139.3 1.1 copy-done
  140.4 0.0 copy-start.1
  140.4 1.7 %copy-done.1 = bf16[2,8,288,192]{3,2,1,0:T(8,128)(2,1)S(1)} copy-done((bf16[2,8,288,192]{3,2,1,0:T(8,128)(2,1)S(1)}, bf16[2,8,288,192]{3,2,1,0:T(8,128)(2,1)}, u32[]{:S(2)}) %copy-start.1) | copy-done | bytes 1769496
  142.1 0.0 copy-start.4
  142.1 0.7 copy-done.4
  142.8 0.0 copy-start.8
  142.8 0.0 copy-start.7
  142.8 0.0 copy-start.6
  142.8 0.0 copy-start.5
  142.8 12.2 %finish.1 = (f32[288,1024]{1,0:T(8,128)}, f32[288,1024]{1,0:T(8,128)}, bf16[2304,1024]{1,0:T(8,128)(2,1)}, bf16[1024,2304]{1,0:T(8,128)(2,1)}) custom-call(f32[4,8,128]{2,1,0:T(8,128)S(1)} %copy-done.4, bf16[8,576,1024]{2,1,0:T(8,128)(2,1)} %get-tuple-element.21.wall_ref, bf16[2,2304,192]{2,1,0:T(8,128)(2,1)S(1)} %bitcast.6, bf16[288,192]{1,0:T(8,128)(2,1)S(1)} %copy-done.2, ...), custom_call_target="tpu_custom_call" | custom-call | tf_op jit(solution)/shard_map/finish/pallas_call | solution.py:417
  155.0 0.0 copy-done.8
  155.0 0.6 copy.24
  155.6 0.0 copy-done.7
  155.6 0.6 copy.25
  156.3 0.0 copy-done.6
  156.3 0.6 copy.26
  156.9 0.0 copy-done.5
  156.9 0.6 copy.27
Async XLA Ops:
  0.6 138.6 %copy-start.2 = (bf16[288,192]{1,0:T(8,128)(2,1)S(1)}, bf16[288,192]{1,0:T(8,128)(2,1)}, u32[]{:S(2)}) copy-start(bf16[288,192]{1,0:T(8,128)(2,1)} %own_v.1) | copy-start | bytes 331780
  0.6 138.6 %copy-start.3 = (bf16[288,192]{1,0:T(8,128)(2,1)S(1)}, bf16[288,192]{1,0:T(8,128)(2,1)}, u32[]{:S(2)}) copy-start(bf16[288,192]{1,0:T(8,128)(2,1)} %own_o.1) | copy-start | bytes 331780
  139.3 1.1 copy-start
  140.4 1.7 %copy-start.1 = (bf16[2,8,288,192]{3,2,1,0:T(8,128)(2,1)S(1)}, bf16[2,8,288,192]{3,2,1,0:T(8,128)(2,1)}, u32[]{:S(2)}) copy-start(bf16[2,8,288,192]{3,2,1,0:T(8,128)(2,1)} %get-tuple-element.22) | copy-start | bytes 5308420
  142.1 0.7 copy-start.4
  142.8 12.2 %copy-start.8 = (f32[24,1024]{1,0:T(8,128)S(1)}, f32[24,1024]{1,0:T(8,128)}, u32[]{:S(2)}) copy-start(f32[24,1024]{1,0:T(8,128)} %get-tuple-element.44) | copy-start | bytes 294916
  142.8 12.8 %copy-start.7 = (f32[24,1024]{1,0:T(8,128)S(1)}, f32[24,1024]{1,0:T(8,128)}, u32[]{:S(2)}) copy-start(f32[24,1024]{1,0:T(8,128)} %get-tuple-element.45) | copy-start | bytes 294916
  142.8 13.5 %copy-start.6 = (f32[24,1024]{1,0:T(8,128)S(1)}, f32[24,1024]{1,0:T(8,128)}, u32[]{:S(2)}) copy-start(f32[24,1024]{1,0:T(8,128)} %get-tuple-element.46) | copy-start | bytes 294916
  142.8 14.1 %copy-start.5 = (f32[24,1024]{1,0:T(8,128)S(1)}, f32[24,1024]{1,0:T(8,128)}, u32[]{:S(2)}) copy-start(f32[24,1024]{1,0:T(8,128)} %get-tuple-element.47) | copy-start | bytes 294916

commit v2 on v1

--- a/solution.py
+++ b/solution.py
@@ -17,8 +17,11 @@
 
 PIECES = 12
 EARLY = 2
-DEPTH = 3
-HOOKS = (3, 5, 6, 12, 17, 22, 27)
+DEPTH = 5
+HOOKS = (3, 5, 8, 16, 23, 30, 34, 37)
+LAG = 3
+UNITS = 2
+STREAMED = 8
 
 
 def adapt(first, second, grad):
@@ -70,8 +73,8 @@
 
 def exchange(
     n, t, x_ref, oc_ref, vc_ref, ret_ref, pv_ref, po_ref, wv_ref, wo_ref, fv_ref, sv_ref, fo_ref, so_ref,
-    wall, pall, dall, sq, nfv, nsv, nfo, nso,
-    xin, pr, gsend, gacross, gpart, grecv,
+    copy_v, copy_o, step_v, step_o, nfv, nsv, nfo, nso,
+    wall, own, pall, xin, cot, old, pr, gsend, gacross, gpart, grecv, dall, dir32, dirs, sq, scales,
     load_sem, p_send, p_recv, x_send, x_recv, core_send, core_recv, ga_send, ga_recv, g_send, g_recv,
     d_send, d_recv, q_send, q_recv, up_send, down_send, over_send, w_recv,
 ):
@@ -85,11 +88,12 @@
     across = me + 1 - 2 * y
     q, columns = wv_ref.shape
     rows = 2 * q
-    rr = fv_ref.shape[0]
+    rr, rank = fv_ref.shape[0], pv_ref.shape[1]
     count, early = cut(rows)
     size = rows // count
     ways = share(q, t)
     part_rows = q // ways
+    streamed = levels <= STREAMED
 
     def remote(src, dst, ssem, rsem, device):
         return pltpu.make_async_remote_copy(
@@ -109,16 +113,31 @@
 
     @pl.when(core == 0)
     def _():
-        pltpu.make_async_copy(x_ref, xin, load_sem).start()
-        pall[0, me] = pv_ref[...]
+        pltpu.make_async_copy(pv_ref, pall.at[0, me], load_sem.at[0]).start()
 
     @pl.when(core == 1)
     def _():
-        pltpu.make_async_copy(oc_ref, xin, load_sem).start()
-        pall[1, me] = po_ref[...]
-
-    wall[me, :q] = wv_ref[...].astype(BF16)
-    wall[me, q:] = wo_ref[...].astype(BF16)
+        pltpu.make_async_copy(po_ref, pall.at[1, me], load_sem.at[0]).start()
+
+    def load(src, dst, k):
+        copy = pltpu.make_async_copy(src, dst, load_sem.at[k])
+        copy.start()
+        return copy
+
+    weights = [load(wv_ref, own.at[0], 1), load(wo_ref, own.at[1], 2)]
+
+    @pl.when(core == 0)
+    def _():
+        pltpu.make_async_copy(x_ref, xin, load_sem.at[3]).start()
+
+    @pl.when(core == 1)
+    def _():
+        pltpu.make_async_copy(oc_ref, xin, load_sem.at[3]).start()
+
+    cots = [load(vc_ref, cot.at[0], 4), load(ret_ref, cot.at[1], 5)]
+    olds = [load(ref, old.at[k], 6 + k) for k, ref in enumerate((fv_ref, sv_ref, fo_ref, so_ref))]
+
+    pltpu.make_async_copy(pv_ref, pall.at[core, me], load_sem.at[0]).wait()
     pl.semaphore_wait(barrier, n - 1 + t - 1)
 
     sends = []
@@ -129,11 +148,11 @@
         return copy
 
     def spread(place, ssem, rsem):
-        own = place(me)
-        first = [go(remote(own, own, ssem.at[0], rsem.at[0], {"fs": across}))]
+        mine = place(me)
+        first = [go(remote(mine, mine, ssem.at[0], rsem.at[0], {"fs": across}))]
         for d in range(1, levels):
             target = lax.rem(z + d, levels) * 2 + y
-            first.append(go(remote(own, own, ssem.at[d], rsem.at[d], {"fs": target})))
+            first.append(go(remote(mine, mine, ssem.at[d], rsem.at[d], {"fs": target})))
         return first
 
     def pass_on(first, place, ssem, rsem):
@@ -154,9 +173,9 @@
 
     def along(slot, step):
         side, s, i = line[slot]
-        place = piece(z - s if step > 0 else z + s, side, i)
+        level = z - s if step > 0 else z + s
+        place = piece(level, side, i)
         ssem = (up_send if step > 0 else down_send).at[slot % DEPTH]
-        level = z - s if step > 0 else z + s
         return remote(place, place, ssem, w_recv.at[side, level, i], {"fs": (z + step) * 2 + y})
 
     def goes(slot, step):
@@ -200,6 +219,11 @@
         @pl.when(z + k < levels)
         def _():
             landed(side, z + k, i)
+
+    def crossed(j, i):
+        if ("over", j, i) not in held:
+            held.add(("over", j, i))
+            landed(1, nearest(j), i)
 
     def drained(slot):
         if 0 <= slot < len(line):
@@ -226,6 +250,54 @@
                 ensure(0, k, i)
             crossing(slot).start()
 
+    copies, steps = (copy_v, copy_o), (step_v, step_o)
+
+    def moved(block, side, low, high):
+        part = jnp.dot(pall[side, block, low:high], dirs[side], preferred_element_type=F32)
+        return part * scales[side, 0:1, 0:1]
+
+    def renew(block, side, low, high):
+        old_part = wall[block, side * q + low:side * q + high].astype(F32)
+        copies[side][block, low:high] = (old_part + moved(block, side, low, high)).astype(BF16)
+
+    def renew_own(side):
+        step = moved(me, side, 0, q)
+        steps[side][...] = step
+        copies[side][me] = (own[side] + step).astype(BF16)
+
+    def unit(side, j, half, low, high):
+        if side == 0 and j == 0:
+            renew_own(half)
+            return
+        for i in range((half * q + low) // size, -(-(half * q + high) // size)):
+            if side == 1 and (i < count - early or j == 0):
+                if i < count - early:
+                    crossed(j, i)
+                else:
+                    ensure(1, 0, i)
+            else:
+                for k in range(1, j + 1):
+                    ensure(side, k, i)
+        renew(nearest(j) * 2 + (y if side == 0 else 1 - y), half, low, high)
+
+    def plan():
+        at_line = {item: slot for slot, item in enumerate(line)}
+        at_over = {item: slot for slot, item in over.items()}
+        units = []
+        for j in range(levels):
+            for side in (0, 1):
+                fine = 2 * size if j == levels - 1 and q % (2 * size) == 0 else q
+                for half in (0, 1):
+                    for low in range(0, q, fine):
+                        ready = 0
+                        for i in range((half * q + low) // size, -(-(half * q + low + fine) // size)):
+                            if side == 1 and (j == 0 or i < count - early):
+                                ready = max(ready, at_over[j, i] + LAG)
+                            elif j > 0:
+                                ready = max(ready, at_line[side, j - 1, i] + LAG)
+                        units.append((ready, len(units), (side, j, half, low, low + fine)))
+        return sorted(units)
+
     chain = {}
 
     def part(block):
@@ -258,13 +330,15 @@
         chain["whole"] = go(
             remote(pall.at[core], pall.at[core], core_send.at[0], core_recv.at[0], {"tp": partner})
         )
-        pltpu.make_async_copy(x_ref, xin, load_sem).wait()
+        pltpu.make_async_copy(x_ref, xin, load_sem.at[3]).wait()
         pr[core] = jnp.dot(xin[...], flat(pall[core]), preferred_element_type=F32).astype(BF16)
         swapped = go(remote(pr.at[core], pr.at[core], core_send.at[1], core_recv.at[1], {"tp": partner}))
+        for copy in cots:
+            copy.wait()
         swapped.wait_recv()
-        for side, cot in ((0, vc_ref), (1, ret_ref)):
+        for side in (0, 1):
             grad = lax.dot_general(
-                pr[side], cot[...], (((0,), (0,)), ((), ())), preferred_element_type=F32
+                pr[side], cot[side], (((0,), (0,)), ((), ())), preferred_element_type=F32
             )
             for peer in range(n):
                 gsend[peer % 2, peer // 2, :, side * columns:(side + 1) * columns] = (
@@ -286,16 +360,18 @@
         chain["g"] = copies
 
     def hook_moments():
+        for copy in olds:
+            copy.wait()
         for copy in chain["g"]:
             copy.wait_recv()
         total = gsend[y, z].astype(F32) + gacross[z].astype(F32)
         for d in range(1, levels):
             total += grecv[lax.rem(z + levels - d, levels)].astype(F32)
-        for side, refs in ((0, (fv_ref, sv_ref, nfv, nsv)), (1, (fo_ref, so_ref, nfo, nso))):
+        for side, refs in ((0, (nfv, nsv)), (1, (nfo, nso))):
             grad = total[:, side * columns:(side + 1) * columns]
-            new_first, new_second, direction = adapt(refs[0][...], refs[1][...], grad)
-            refs[2][...] = new_first
-            refs[3][...] = new_second
+            new_first, new_second, direction = adapt(old[2 * side], old[2 * side + 1], grad)
+            refs[0][...] = new_first
+            refs[1][...] = new_second
             dall[me, :, side * columns:(side + 1) * columns] = direction
         chain["dirs"] = spread(lambda block: dall.at[block], d_send, d_recv)
 
@@ -307,10 +383,11 @@
             copy.wait_recv()
         sums = []
         for side in (0, 1):
-            acc = jnp.zeros((rr, columns), F32)
             for k in range(n):
-                acc += jnp.square(dall[k, :, side * columns:(side + 1) * columns].astype(F32))
-            sums.append(jnp.sum(acc))
+                dir32[k * rr:(k + 1) * rr] = dall[k, :, side * columns:(side + 1) * columns].astype(F32)
+            whole = dir32[...]
+            sums.append(jnp.sum(jnp.square(whole)))
+            dirs[side] = whole.astype(BF16)
         row = lax.broadcasted_iota(jnp.int32, sq.shape[1:], 0)
         sq[tp] = jnp.where(row == 0, sums[0], sums[1])
         chain["sq"] = [
@@ -318,16 +395,35 @@
             for d in range(1, t)
         ]
 
-    hooks = dict(zip(
-        HOOKS, (hook_pass, hook_share, hook_grads, hook_partial, hook_moments, hook_dirs, hook_sums)
-    ))
+    def hook_scales():
+        for copy in chain["sq"]:
+            copy.wait_recv()
+        chain["whole"].wait_recv()
+        totals = jnp.sum(sq[...], axis=0)
+        spread_scales = lax.rsqrt(totals / float(rank * columns * t) + norm_eps)
+        for side in (0, 1):
+            scales[side] = jnp.broadcast_to(spread_scales[side:side + 1], scales.shape[1:])
+
+    hooks = dict(zip(HOOKS, (
+        hook_pass, hook_share, hook_grads, hook_partial, hook_moments, hook_dirs, hook_sums, hook_scales
+    )))
     chain["shared"] = []
     chain["proj"] = spread(part, p_send, p_recv)
+    for side in (0, 1):
+        weights[side].wait()
+        wall[me, side * q:(side + 1) * q] = own[side].astype(BF16)
+    units = plan() if streamed else []
     end = max(slots, max(HOOKS) + 1)
     for slot in range(end):
         if slot in hooks:
             hooks[slot]()
         advance(slot)
+        if slot >= max(HOOKS):
+            for _ in range(UNITS):
+                if units and units[0][0] <= slot:
+                    unit(*units.pop(0)[2])
+    for _, _, args in units:
+        unit(*args)
     for slot in range(end, slots + DEPTH):
         drained(slot - DEPTH)
 
@@ -336,31 +432,46 @@
             ensure(0, k, i)
         for i in range(count - early, count):
             ensure(1, k, i)
+    for i in range(count - early, count):
+        ensure(1, 0, i)
     for j in range(levels):
         for i in range(count - early):
-            landed(1, nearest(j), i)
-    for copy in chain["sq"]:
-        copy.wait_recv()
-    chain["whole"].wait_recv()
+            crossed(j, i)
+    if not streamed:
+        def whole_block(block, carry):
+            for side in (0, 1):
+                renew(block, side, 0, q)
+            return carry
+
+        lax.fori_loop(0, n, whole_block, 0)
+        for side in (0, 1):
+            renew_own(side)
     for copy in sends:
         copy.wait_send()
 
 
-def finish(q, count, sq_ref, wall_ref, pall_ref, own_v, own_o, dv_ref, do_ref, step_v, step_o, copy_v, copy_o):
-    totals = jnp.sum(sq_ref[...], axis=0)
-    scale_v = lax.rsqrt(totals[0:1, 0:1] / count + norm_eps)
-    scale_o = lax.rsqrt(totals[1:2, 0:1] / count + norm_eps)
-    n, _, lanes = wall_ref.shape
-    dir_v, dir_o = dv_ref[...], do_ref[...]
-    step_v[...] = jnp.dot(own_v[...], dir_v, preferred_element_type=F32) * scale_v
-    step_o[...] = jnp.dot(own_o[...], dir_o, preferred_element_type=F32) * scale_o
-    w_v = wall_ref[:, :q].astype(F32).reshape(n * q, lanes)
-    w_o = wall_ref[:, q:].astype(F32).reshape(n * q, lanes)
-    copy_v[...] = (
-        w_v + jnp.dot(pall_ref[0], dir_v, preferred_element_type=F32) * scale_v
-    ).astype(BF16)
-    moved = w_o + jnp.dot(pall_ref[1], dir_o, preferred_element_type=F32) * scale_o
-    copy_o[...] = moved.T.astype(BF16)
+def finish(
+    o_ref, v_ref, step_v, step_o, nfv, nsv, nfo, nso,
+    copy_o, copy_v, out_v, out_o, first_v, second_v, first_o, second_o, sem,
+):
+    pairs = (
+        (v_ref, copy_v), (step_v, out_v), (step_o, out_o),
+        (nfv, first_v), (nsv, second_v), (nfo, first_o), (nso, second_o),
+    )
+    copies = [pltpu.make_async_copy(src, dst, sem.at[k]) for k, (src, dst) in enumerate(pairs)]
+
+    @pl.when(pl.program_id(0) == 0)
+    def _():
+        for copy in copies:
+            copy.start()
+
+    parts, q, lanes = o_ref.shape
+    copy_o[...] = o_ref[...].astype(F32).reshape(parts * q, lanes).T.astype(BF16)
+
+    @pl.when(pl.program_id(0) == pl.num_programs(0) - 1)
+    def _():
+        for copy in copies:
+            copy.wait()
 
 
 def per_device(
@@ -375,72 +486,73 @@
     levels = n // 2
     pieces, _ = cut(2 * q)
     ways = share(q, t)
+    hbm = pl.BlockSpec(memory_space=pltpu.HBM)
     vmem = pl.BlockSpec(memory_space=pltpu.VMEM)
     anywhere = pl.BlockSpec(memory_space=pl.ANY)
     dma = pltpu.SemaphoreType.DMA
-    moment = jax.ShapeDtypeStruct((rr, columns), F32)
-    wall, pall, dall, sq, first_v, second_v, first_o, second_o = pl.pallas_call(
+    results = pl.pallas_call(
         functools.partial(exchange, n, t),
         out_shape=(
-            jax.ShapeDtypeStruct((n, 2 * q, columns), BF16),
-            jax.ShapeDtypeStruct((2, n, q, rank), BF16),
-            jax.ShapeDtypeStruct((n, rr, 2 * columns), BF16),
-            jax.ShapeDtypeStruct((t, 8, 128), F32),
-            moment, moment, moment, moment,
+            pltpu.VMEM((n, q, columns), BF16),
+            pltpu.VMEM((n, q, columns), BF16),
+            pltpu.VMEM((q, columns), F32),
+            pltpu.VMEM((q, columns), F32),
+            pltpu.VMEM((rr, columns), F32),
+            pltpu.VMEM((rr, columns), F32),
+            pltpu.VMEM((rr, columns), F32),
+            pltpu.VMEM((rr, columns), F32),
         ),
-        in_specs=[anywhere, anywhere] + [vmem] * 10,
+        in_specs=[hbm] * 12,
         out_specs=(vmem,) * 8,
         scratch_shapes=[
+            pltpu.VMEM((n, 2 * q, columns), BF16),
+            pltpu.VMEM((2, q, columns), F32),
+            pltpu.VMEM((2, n, q, rank), BF16),
             pltpu.VMEM((tokens, width), BF16),
+            pltpu.VMEM((2, tokens, columns), BF16),
+            pltpu.VMEM((4, rr, columns), F32),
             pltpu.VMEM((2, tokens, rank), BF16),
             pltpu.VMEM((2, levels, rr, 2 * columns), BF16),
             pltpu.VMEM((levels, rr, 2 * columns), BF16),
             pltpu.VMEM((levels, rr, 2 * columns), BF16),
             pltpu.VMEM((levels, rr, 2 * columns), BF16),
-            dma, dma((n,)), dma((n,)), dma((ways, n)), dma((ways, n)), dma((2,)), dma((2,)),
+            pltpu.VMEM((n, rr, 2 * columns), BF16),
+            pltpu.VMEM((rank, columns), F32),
+            pltpu.VMEM((2, rank, columns), BF16),
+            pltpu.VMEM((t, 8, 128), F32),
+            pltpu.VMEM((2, 8, 128), F32),
+            dma((10,)), dma((n,)), dma((n,)), dma((ways, n)), dma((ways, n)), dma((2,)), dma((2,)),
             dma((1,)), dma((1,)), dma((levels,)), dma((levels,)), dma((n,)), dma((n,)),
             dma((t,)), dma((t,)),
             dma((DEPTH,)), dma((DEPTH,)), dma((DEPTH,)), dma((2, levels, pieces)),
         ],
         compiler_params=pltpu.CompilerParams(
-            collective_id=0, has_side_effects=True, vmem_limit_bytes=60 * 1024 * 1024
+            collective_id=0, has_side_effects=True, vmem_limit_bytes=51 * 1024 * 1024
         ),
         name="exchange",
     )(
         inputs, output_cot, value_cot, retained, proj_value, proj_output, w_value, w_output.T,
         first_value, second_value, first_output, second_output,
     )
+    copy_v, copy_o, step_v, step_o = results[:4]
     lanes = 128
-    tiles = columns // lanes
-    dirs = dall.reshape(n * rr, 2 * columns)
     full = n * q
-    step_v, step_o, copy_v, copy_o = pl.pallas_call(
-        functools.partial(finish, q, float(rank * columns * t)),
-        grid=(tiles,),
+    step = jax.ShapeDtypeStruct((q, columns), F32)
+    moment = jax.ShapeDtypeStruct((rr, columns), F32)
+    copy_o, copy_v, step_v, step_o, first_v, second_v, first_o, second_o = pl.pallas_call(
+        finish,
+        grid=(columns // lanes,),
         out_shape=(
-            jax.ShapeDtypeStruct((q, columns), F32),
-            jax.ShapeDtypeStruct((q, columns), F32),
+            jax.ShapeDtypeStruct((columns, full), BF16),
             jax.ShapeDtypeStruct((full, columns), BF16),
-            jax.ShapeDtypeStruct((columns, full), BF16),
+            step, step, moment, moment, moment, moment,
         ),
-        in_specs=[
-            pl.BlockSpec((t, 8, 128), lambda j: (0, 0, 0)),
-            pl.BlockSpec((n, 2 * q, lanes), lambda j: (0, 0, j)),
-            pl.BlockSpec((2, full, rank), lambda j: (0, 0, 0)),
-            pl.BlockSpec((q, rank), lambda j: (0, 0)),
-            pl.BlockSpec((q, rank), lambda j: (0, 0)),
-            pl.BlockSpec((rank, lanes), lambda j: (0, j)),
-            pl.BlockSpec((rank, lanes), lambda j: (0, j + tiles)),
-        ],
-        out_specs=(
-            pl.BlockSpec((q, lanes), lambda j: (0, j)),
-            pl.BlockSpec((q, lanes), lambda j: (0, j)),
-            pl.BlockSpec((full, lanes), lambda j: (0, j)),
-            pl.BlockSpec((lanes, full), lambda j: (j, 0)),
-        ),
-        compiler_params=pltpu.CompilerParams(vmem_limit_bytes=48 * 1024 * 1024),
+        in_specs=[pl.BlockSpec((n, q, lanes), lambda j: (0, 0, j))] + [anywhere] * 7,
+        out_specs=(pl.BlockSpec((lanes, full), lambda j: (j, 0)),) + (anywhere,) * 7,
+        scratch_shapes=[dma((7,))],
+        compiler_params=pltpu.CompilerParams(vmem_limit_bytes=12 * 1024 * 1024),
         name="finish",
-    )(sq, wall, pall.reshape(2, full, rank), proj_value, proj_output, dirs, dirs)
+    )(copy_o, copy_v.reshape(full, columns), step_v, step_o, *results[4:])
     return (step_v, step_o.T, copy_v, copy_o, first_v, second_v, first_o, second_o)
 
 

time: 158 us -> 129 us (0.82)
  Pallas kernels: 151 us -> 128 us
  local copies, waits for them, and re-layouts: 6.09 us -> 0 us
    pallas_call x2, Pallas kernels: 151 us -> 128 us  [the longest x1 120 us: per_device(): pl.pallas_call(functools.partial(exchange, n, t), out_shape=(pltpu.VMEM((...]
    unnamed x22 -> x0, local copies, waits for them, and re-layouts: 6.09 us -> none
where the time goes in v2:
time: 129 us; the launch traced here: 128 us
  Pallas kernels  128 us (99%)
    pallas_call x1, Pallas kernels, per_device(): pl.pallas_call(functools.partial(exchange, n, t), out_shape=(pltpu.VMEM((...  120 us
    pallas_call x1, Pallas kernels, per_device(): pl.pallas_call(finish, grid=(columns // lanes,), out_shape=(jax.ShapeDtyp...  7.5 us

profile of v2, /device:TPU:13, one launch (start us, length us, event | category | flops | bytes accessed | tf_op | source)
XLA Modules:
  0.0 128.3 jit_solution(9319133073251600804)
XLA Ops:
  0.6 120.1 %exchange.1 = (bf16[8,288,1024]{2,1,0:T(8,128)(2,1)S(1)}, bf16[8,288,1024]{2,1,0:T(8,128)(2,1)S(1)}, f32[288,1024]{1,0:T(8,128)S(1)}, f32[288,1024]{1,0:T(8,128)...) custom-call(bf16[512,2304]{1,0:T(8,128)(2,1)} %x_ref.1, ...), custom_call_target="tpu_custom_call" | custom-call | tf_op jit(solution)/shard_map/exchange/pallas_call | solution.py:493
  120.8 7.5 %finish.1 = (bf16[1024,2304]{1,0:T(8,128)(2,1)}, bf16[2304,1024]{1,0:T(8,128)(2,1)}, f32[288,1024]{1,0:T(8,128)}, f32[288,1024]{1,0:T(8,128)}, f32[24,1024]{1,0:...) custom-call(bf16[8,288,1024]{2,1,0:T(8,128)(2,1)S(1)} %get-tuple-element.24.o_ref, ...), custom_call_target="tpu_custom_call" | custom-call | tf_op jit(solution)/shard_map/finish/pallas_call | solution.py:542

commit v3 on v2

--- a/solution.py
+++ b/solution.py
@@ -20,7 +20,10 @@
 DEPTH = 5
 HOOKS = (3, 5, 8, 16, 23, 30, 34, 37)
 LAG = 3
-UNITS = 2
+UNITS = 4
+LANES = 128
+DEEP = 12
+SPLIT = 2
 STREAMED = 8
 
 
@@ -74,8 +77,8 @@
 def exchange(
     n, t, x_ref, oc_ref, vc_ref, ret_ref, pv_ref, po_ref, wv_ref, wo_ref, fv_ref, sv_ref, fo_ref, so_ref,
     copy_v, copy_o, step_v, step_o, nfv, nsv, nfo, nso,
-    wall, own, pall, xin, cot, old, pr, gsend, gacross, gpart, grecv, dall, dir32, dirs, sq, scales,
-    load_sem, p_send, p_recv, x_send, x_recv, core_send, core_recv, ga_send, ga_recv, g_send, g_recv,
+    wall, flip, own, pall, xin, cot, old, pr, gsend, grecv, gpart, gfin, total, dall, dir32, dirs, sq, scales,
+    load_sem, p_send, p_recv, x_send, x_recv, core_send, core_recv, g_send, g_recv, f_send, f_recv,
     d_send, d_recv, q_send, q_recv, up_send, down_send, over_send, w_recv,
 ):
     me = lax.axis_index("fs")
@@ -94,6 +97,8 @@
     ways = share(q, t)
     part_rows = q // ways
     streamed = levels <= STREAMED
+    paired = levels == 4 and 4 * q % LANES == 0
+    base = (q, 0)
 
     def remote(src, dst, ssem, rsem, device):
         return pltpu.make_async_remote_copy(
@@ -175,7 +180,7 @@
         side, s, i = line[slot]
         level = z - s if step > 0 else z + s
         place = piece(level, side, i)
-        ssem = (up_send if step > 0 else down_send).at[slot % DEPTH]
+        ssem = (up_send if step > 0 else down_send).at[slot % DEEP]
         return remote(place, place, ssem, w_recv.at[side, level, i], {"fs": (z + step) * 2 + y})
 
     def goes(slot, step):
@@ -225,17 +230,23 @@
             held.add(("over", j, i))
             landed(1, nearest(j), i)
 
+    def tight(step):
+        return z + step == (levels - 1 if step > 0 else 0)
+
     def drained(slot):
-        if 0 <= slot < len(line):
-            for step in (1, -1):
-                @pl.when(goes(slot, step))
-                def _():
-                    along(slot, step).wait_send()
-        if slot in over:
-            crossing(slot).wait_send()
+        for depth in (DEPTH, DEEP):
+            if 0 <= slot - depth < len(line):
+                for step in (1, -1):
+                    close = tight(step) if depth == DEPTH else jnp.logical_not(tight(step))
+
+                    @pl.when(jnp.logical_and(goes(slot - depth, step), close))
+                    def _():
+                        along(slot - depth, step).wait_send()
+        if slot - DEPTH in over:
+            crossing(slot - DEPTH).wait_send()
 
     def advance(slot):
-        drained(slot - DEPTH)
+        drained(slot)
         if slot < len(line):
             side, s, i = line[slot]
             if side == 1 or s > 0:
@@ -250,26 +261,37 @@
                 ensure(0, k, i)
             crossing(slot).start()
 
-    copies, steps = (copy_v, copy_o), (step_v, step_o)
+    steps = (step_v, step_o)
+
+    def keep(block, side, low, high, value):
+        if side == 0:
+            copy_v[block, low:high] = value.astype(BF16)
+        else:
+            flip[block, low:high] = value.astype(BF16)
+
+    def turn(chunk):
+        start = pl.multiple_of(chunk * LANES, LANES)
+        tile = flip.reshape(n * q, columns)[pl.ds(start, LANES)]
+        copy_o[:, pl.ds(start, LANES)] = tile.astype(F32).T.astype(BF16)
 
     def moved(block, side, low, high):
         part = jnp.dot(pall[side, block, low:high], dirs[side], preferred_element_type=F32)
         return part * scales[side, 0:1, 0:1]
 
     def renew(block, side, low, high):
-        old_part = wall[block, side * q + low:side * q + high].astype(F32)
-        copies[side][block, low:high] = (old_part + moved(block, side, low, high)).astype(BF16)
+        old_part = wall[block, base[side] + low:base[side] + high].astype(F32)
+        keep(block, side, low, high, old_part + moved(block, side, low, high))
 
     def renew_own(side):
         step = moved(me, side, 0, q)
         steps[side][...] = step
-        copies[side][me] = (own[side] + step).astype(BF16)
+        keep(me, side, 0, q, own[side] + step)
 
     def unit(side, j, half, low, high):
         if side == 0 and j == 0:
             renew_own(half)
             return
-        for i in range((half * q + low) // size, -(-(half * q + high) // size)):
+        for i in range((base[half] + low) // size, -(-(base[half] + high) // size)):
             if side == 1 and (i < count - early or j == 0):
                 if i < count - early:
                     crossed(j, i)
@@ -283,20 +305,40 @@
     def plan():
         at_line = {item: slot for slot, item in enumerate(line)}
         at_over = {item: slot for slot, item in over.items()}
-        units = []
+        units, flipped = [], [0] * levels
+
+        def add(ready, work, *args):
+            units.append((ready, len(units), work, args))
+
         for j in range(levels):
-            for side in (0, 1):
-                fine = 2 * size if j == levels - 1 and q % (2 * size) == 0 else q
-                for half in (0, 1):
+            for half in (1, 0):
+                for side in (0, 1):
+                    fine = 2 * size if j == levels - 1 and q % (2 * size) == 0 else q
                     for low in range(0, q, fine):
-                        ready = 0
-                        for i in range((half * q + low) // size, -(-(half * q + low + fine) // size)):
+                        ready, start = 0, base[half] + low
+                        for i in range(start // size, -(-(start + fine) // size)):
                             if side == 1 and (j == 0 or i < count - early):
                                 ready = max(ready, at_over[j, i] + LAG)
                             elif j > 0:
                                 ready = max(ready, at_line[side, j - 1, i] + LAG)
-                        units.append((ready, len(units), (side, j, half, low, low + fine)))
-        return sorted(units)
+                        if half == 1:
+                            flipped[j] = max(flipped[j], ready)
+                        add(ready, unit, side, j, half, low, low + fine)
+            if paired and j >= 2:
+                group = 4 * q // LANES
+                near = z // 2
+                low = jnp.where(z < 2, 0, 1)
+                split = 2 * q // LANES
+                rest = group - split
+                if j == 2:
+                    for c in range(group):
+                        add(max(flipped[:3]), turn, near * group + c)
+                    for c in range(split):
+                        add(max(flipped[:3]), turn, (1 - near) * group + low * rest + c)
+                else:
+                    for c in range(rest):
+                        add(max(flipped), turn, (1 - near) * group + (1 - low) * split + c)
+        return sorted(units, key=lambda item: item[:2])
 
     chain = {}
 
@@ -341,32 +383,96 @@
                 pr[side], cot[side], (((0,), (0,)), ((), ())), preferred_element_type=F32
             )
             for peer in range(n):
-                gsend[peer % 2, peer // 2, :, side * columns:(side + 1) * columns] = (
+                gsend[peer // 2, peer % 2, :, side * columns:(side + 1) * columns] = (
                     grad[peer * rr:(peer + 1) * rr].astype(BF16)
                 )
-        chain["ga"] = go(
-            remote(gsend.at[1 - y], gacross, ga_send.at[0], ga_recv.at[0], {"fs": across})
-        )
+        for d in range(1, levels):
+            scatter(d, "start")
+        final(ends, gsend.at[z, 1 - y], 0, across, "start")
+
+    inside = jnp.logical_and(z > 0, z < levels - 1) if levels > 3 else z >= 0
+    ends = jnp.logical_not(inside)
+
+    def scatter(d, act):
+        level = lax.rem(z + d, levels)
+
+        def send(kind, owner):
+            copy = remote(
+                gsend.at[level], grecv.at[kind, z], g_send.at[d], g_recv.at[kind, z], {"fs": owner * 2 + y}
+            )
+            copy.start() if act == "start" else copy.wait_send()
+
+        if levels < 4:
+            send(0, level)
+            return
+        inner = jnp.logical_and(level > 0, level < levels - 1)
+        owner = jnp.where(level == 0, 1, levels - 2)
+
+        @pl.when(inner)
+        def _():
+            send(0, level)
+
+        @pl.when(jnp.logical_and(jnp.logical_not(inner), z != owner))
+        def _():
+            send(1, owner)
+
+    def final(when, src, k, peer, act):
+        @pl.when(when)
+        def _():
+            copy = remote(src, gfin.at[k], f_send.at[k], f_recv.at[k], {"fs": peer})
+            copy.start() if act == "start" else copy.wait_send()
+
+    def arrived(kind, d):
+        level = lax.rem(z + d, levels)
+        place = grecv.at[kind, level]
+        remote(place, place, g_send.at[d], g_recv.at[kind, level], {"fs": across}).wait_recv()
+        return place[...].astype(F32)
+
+    def finals(act):
+        final(inside, gpart.at[0, 1 - y], 0, across, act)
+        if levels > 3:
+            for own_level, end in ((1, 0), (levels - 2, levels - 1)):
+                final(z == own_level, gpart.at[1, y], 1, end * 2 + y, act)
+                final(z == own_level, gpart.at[1, 1 - y], 2, end * 2 + 1 - y, act)
 
     def hook_partial():
-        chain["ga"].wait_recv()
-        gpart[...] = (gsend[y].astype(F32) + gacross[...].astype(F32)).astype(BF16)
-        copies = []
-        for d in range(1, levels):
-            level = lax.rem(z + d, levels)
-            copies.append(
-                go(remote(gpart.at[level], grecv.at[z], g_send.at[d], g_recv.at[d], {"fs": level * 2 + y}))
-            )
-        chain["g"] = copies
+        @pl.when(inside)
+        def _():
+            summed = gsend[z].astype(F32)
+            for d in range(1, levels):
+                summed += arrived(0, d)
+            gpart[0] = summed.astype(BF16)
+
+        if levels > 3:
+            for own_level, end, sources in (
+                (1, 0, range(1, levels - 1)), (levels - 2, levels - 1, range(2, levels))
+            ):
+                @pl.when(z == own_level)
+                def _():
+                    summed = gsend[end].astype(F32)
+                    for d in sources:
+                        summed += arrived(1, d)
+                    gpart[1] = summed.astype(BF16)
+
+        finals("start")
 
     def hook_moments():
         for copy in olds:
             copy.wait()
-        for copy in chain["g"]:
-            copy.wait_recv()
-        total = gsend[y, z].astype(F32) + gacross[z].astype(F32)
-        for d in range(1, levels):
-            total += grecv[lax.rem(z + levels - d, levels)].astype(F32)
+
+        def fetched(k):
+            remote(gfin.at[k], gfin.at[k], f_send.at[k], f_recv.at[k], {"fs": across}).wait_recv()
+            return gfin[k].astype(F32)
+
+        @pl.when(inside)
+        def _():
+            total[...] = gpart[0, y].astype(F32) + fetched(0)
+
+        if levels > 3:
+            @pl.when(ends)
+            def _():
+                total[...] = gsend[z, y].astype(F32) + fetched(0) + fetched(1) + fetched(2)
+
         for side, refs in ((0, (nfv, nsv)), (1, (nfo, nso))):
             grad = total[:, side * columns:(side + 1) * columns]
             new_first, new_second, direction = adapt(old[2 * side], old[2 * side + 1], grad)
@@ -411,7 +517,7 @@
     chain["proj"] = spread(part, p_send, p_recv)
     for side in (0, 1):
         weights[side].wait()
-        wall[me, side * q:(side + 1) * q] = own[side].astype(BF16)
+        wall[me, base[side]:base[side] + q] = own[side].astype(BF16)
     units = plan() if streamed else []
     end = max(slots, max(HOOKS) + 1)
     for slot in range(end):
@@ -421,11 +527,12 @@
         if slot >= max(HOOKS):
             for _ in range(UNITS):
                 if units and units[0][0] <= slot:
-                    unit(*units.pop(0)[2])
-    for _, _, args in units:
-        unit(*args)
-    for slot in range(end, slots + DEPTH):
-        drained(slot - DEPTH)
+                    _, _, work, args = units.pop(0)
+                    work(*args)
+    for _, _, work, args in units:
+        work(*args)
+    for slot in range(end, slots + DEEP):
+        drained(slot)
 
     for k in range(1, levels):
         for i in range(count):
@@ -446,32 +553,33 @@
         lax.fori_loop(0, n, whole_block, 0)
         for side in (0, 1):
             renew_own(side)
+    if not (streamed and paired):
+        def one_chunk(chunk, carry):
+            turn(chunk)
+            return carry
+
+        lax.fori_loop(0, n * q // LANES, one_chunk, 0)
     for copy in sends:
         copy.wait_send()
-
-
-def finish(
-    o_ref, v_ref, step_v, step_o, nfv, nsv, nfo, nso,
-    copy_o, copy_v, out_v, out_o, first_v, second_v, first_o, second_o, sem,
-):
-    pairs = (
-        (v_ref, copy_v), (step_v, out_v), (step_o, out_o),
-        (nfv, first_v), (nsv, second_v), (nfo, first_o), (nso, second_o),
-    )
-    copies = [pltpu.make_async_copy(src, dst, sem.at[k]) for k, (src, dst) in enumerate(pairs)]
-
-    @pl.when(pl.program_id(0) == 0)
-    def _():
-        for copy in copies:
-            copy.start()
-
-    parts, q, lanes = o_ref.shape
-    copy_o[...] = o_ref[...].astype(F32).reshape(parts * q, lanes).T.astype(BF16)
-
-    @pl.when(pl.program_id(0) == pl.num_programs(0) - 1)
-    def _():
-        for copy in copies:
-            copy.wait()
+    for d in range(1, levels):
+        scatter(d, "wait")
+    final(ends, gsend.at[z, 1 - y], 0, across, "wait")
+    finals("wait")
+
+
+def finish(*refs):
+    sem, count = refs[-1], len(refs) // 2
+    copies = []
+    for src, dst in zip(refs[:count], refs[count:]):
+        rows = src.shape[0]
+        parts = SPLIT if rows % (16 * SPLIT) == 0 else 1
+        for p in range(parts):
+            place = pl.ds(p * (rows // parts), rows // parts)
+            copies.append(pltpu.make_async_copy(src.at[place], dst.at[place], sem.at[len(copies)]))
+    for copy in copies:
+        copy.start()
+    for copy in copies:
+        copy.wait()
 
 
 def per_device(
@@ -494,7 +602,7 @@
         functools.partial(exchange, n, t),
         out_shape=(
             pltpu.VMEM((n, q, columns), BF16),
-            pltpu.VMEM((n, q, columns), BF16),
+            pltpu.VMEM((columns, n * q), BF16),
             pltpu.VMEM((q, columns), F32),
             pltpu.VMEM((q, columns), F32),
             pltpu.VMEM((rr, columns), F32),
@@ -506,25 +614,27 @@
         out_specs=(vmem,) * 8,
         scratch_shapes=[
             pltpu.VMEM((n, 2 * q, columns), BF16),
+            pltpu.VMEM((n, q, columns), BF16),
             pltpu.VMEM((2, q, columns), F32),
             pltpu.VMEM((2, n, q, rank), BF16),
             pltpu.VMEM((tokens, width), BF16),
             pltpu.VMEM((2, tokens, columns), BF16),
             pltpu.VMEM((4, rr, columns), F32),
             pltpu.VMEM((2, tokens, rank), BF16),
-            pltpu.VMEM((2, levels, rr, 2 * columns), BF16),
-            pltpu.VMEM((levels, rr, 2 * columns), BF16),
-            pltpu.VMEM((levels, rr, 2 * columns), BF16),
-            pltpu.VMEM((levels, rr, 2 * columns), BF16),
+            pltpu.VMEM((levels, 2, rr, 2 * columns), BF16),
+            pltpu.VMEM((2, levels, 2, rr, 2 * columns), BF16),
+            pltpu.VMEM((2, 2, rr, 2 * columns), BF16),
+            pltpu.VMEM((3, rr, 2 * columns), BF16),
+            pltpu.VMEM((rr, 2 * columns), F32),
             pltpu.VMEM((n, rr, 2 * columns), BF16),
             pltpu.VMEM((rank, columns), F32),
             pltpu.VMEM((2, rank, columns), BF16),
             pltpu.VMEM((t, 8, 128), F32),
             pltpu.VMEM((2, 8, 128), F32),
             dma((10,)), dma((n,)), dma((n,)), dma((ways, n)), dma((ways, n)), dma((2,)), dma((2,)),
-            dma((1,)), dma((1,)), dma((levels,)), dma((levels,)), dma((n,)), dma((n,)),
+            dma((levels,)), dma((2, levels)), dma((3,)), dma((3,)), dma((n,)), dma((n,)),
             dma((t,)), dma((t,)),
-            dma((DEPTH,)), dma((DEPTH,)), dma((DEPTH,)), dma((2, levels, pieces)),
+            dma((DEEP,)), dma((DEEP,)), dma((DEPTH,)), dma((2, levels, pieces)),
         ],
         compiler_params=pltpu.CompilerParams(
             collective_id=0, has_side_effects=True, vmem_limit_bytes=51 * 1024 * 1024
@@ -534,25 +644,17 @@
         inputs, output_cot, value_cot, retained, proj_value, proj_output, w_value, w_output.T,
         first_value, second_value, first_output, second_output,
     )
-    copy_v, copy_o, step_v, step_o = results[:4]
-    lanes = 128
     full = n * q
-    step = jax.ShapeDtypeStruct((q, columns), F32)
-    moment = jax.ShapeDtypeStruct((rr, columns), F32)
-    copy_o, copy_v, step_v, step_o, first_v, second_v, first_o, second_o = pl.pallas_call(
+    values = (results[0].reshape(full, columns),) + tuple(results[1:])
+    copy_v, copy_o, step_v, step_o, first_v, second_v, first_o, second_o = pl.pallas_call(
         finish,
-        grid=(columns // lanes,),
-        out_shape=(
-            jax.ShapeDtypeStruct((columns, full), BF16),
-            jax.ShapeDtypeStruct((full, columns), BF16),
-            step, step, moment, moment, moment, moment,
-        ),
-        in_specs=[pl.BlockSpec((n, q, lanes), lambda j: (0, 0, j))] + [anywhere] * 7,
-        out_specs=(pl.BlockSpec((lanes, full), lambda j: (j, 0)),) + (anywhere,) * 7,
-        scratch_shapes=[dma((7,))],
+        out_shape=tuple(jax.ShapeDtypeStruct(value.shape, value.dtype) for value in values),
+        in_specs=[anywhere] * 8,
+        out_specs=(anywhere,) * 8,
+        scratch_shapes=[dma((8 * SPLIT,))],
         compiler_params=pltpu.CompilerParams(vmem_limit_bytes=12 * 1024 * 1024),
         name="finish",
-    )(copy_o, copy_v.reshape(full, columns), step_v, step_o, *results[4:])
+    )(*values)
     return (step_v, step_o.T, copy_v, copy_o, first_v, second_v, first_o, second_o)
 
 

time: 129 us -> 125 us (0.969)
  Pallas kernels: 128 us -> 122 us
    pallas_call x1, Pallas kernels: 7.5 us -> 4.56 us  [per_device(): pl.pallas_call(finish, out_shape=tuple((jax.ShapeDtypeStruct(value.shape,...]
    pallas_call x1, Pallas kernels: 120 us -> 118 us  [per_device(): pl.pallas_call(functools.partial(exchange, n, t), out_shape=(pltpu.VMEM((...]
where the time goes in v3:
time: 125 us; the launch traced here: 123 us
  Pallas kernels  122 us (98%)
    pallas_call x1, Pallas kernels, per_device(): pl.pallas_call(functools.partial(exchange, n, t), out_shape=(pltpu.VMEM((...  118 us
    pallas_call x1, Pallas kernels, per_device(): pl.pallas_call(finish, out_shape=tuple((jax.ShapeDtypeStruct(value.shape,...  4.56 us

profile of v3, /device:TPU:13, one launch (start us, length us, event | category | flops | bytes accessed | tf_op | source)
XLA Modules:
  0.0 123.1 jit_solution(7989436995088404788)
XLA Ops:
  0.6 117.9 %exchange.1 = (bf16[8,288,1024]{2,1,0:T(8,128)(2,1)S(1)}, bf16[1024,2304]{1,0:T(8,128)(2,1)S(1)}, f32[288,1024]{1,0:T(8,128)S(1)}, f32[288,1024]{1,0:T(8,128)S(1...) custom-call(bf16[512,2304]{1,0:T(8,128)(2,1)} %x_ref.1, ...), custom_call_target="tpu_custom_call" | custom-call | tf_op jit(solution)/shard_map/exchange/pallas_call | solution.py:601
  118.5 4.6 %finish.1 = (bf16[2304,1024]{1,0:T(8,128)(2,1)}, bf16[1024,2304]{1,0:T(8,128)(2,1)}, f32[288,1024]{1,0:T(8,128)}, f32[288,1024]{1,0:T(8,128)}, f32[24,1024]{1,0:...) custom-call(bf16[2304,1024]{1,0:T(8,128)(2,1)S(1)} %bitcast.3, ...), custom_call_target="tpu_custom_call" | custom-call | tf_op jit(solution)/shard_map/finish/pallas_call | solution.py:649

commit v4 on v3

--- a/solution.py
+++ b/solution.py
@@ -16,13 +16,14 @@
 norm_eps = 1e-06
 
 PIECES = 12
-EARLY = 2
+SHARE = 0.2
 DEPTH = 5
-HOOKS = (3, 5, 8, 16, 23, 30, 34, 37)
+HOOKS = (2, 5, 11, 12, 13, 20, 25, 31, 36)
 LAG = 3
 UNITS = 4
 LANES = 128
 DEEP = 12
+LATE = 1
 SPLIT = 2
 STREAMED = 8
 
@@ -43,9 +44,11 @@
 
 def cut(rows):
     if rows % (16 * PIECES) == 0:
-        return PIECES, EARLY
-    count = rows // 16
-    return count, max(1, count * EARLY // PIECES)
+        ahead = max(32, int(rows * SHARE) // 16 * 16)
+        late, size = rows - ahead, rows // PIECES
+        return list(range(0, late, size)) + [late, late + ahead // 32 * 16, rows], 2
+    edges = list(range(0, rows + 1, 16))
+    return edges, max(1, int((len(edges) - 1) * SHARE))
 
 
 def share(q, t):
@@ -77,9 +80,9 @@
 def exchange(
     n, t, x_ref, oc_ref, vc_ref, ret_ref, pv_ref, po_ref, wv_ref, wo_ref, fv_ref, sv_ref, fo_ref, so_ref,
     copy_v, copy_o, step_v, step_o, nfv, nsv, nfo, nso,
-    wall, flip, own, pall, xin, cot, old, pr, gsend, grecv, gpart, gfin, total, dall, dir32, dirs, sq, scales,
+    wall, flip, own, pall, xin, cot, old, pr, gsend, grecv, gpart, gfin, total, dall, dir32, dirs, sq, fsq, scales,
     load_sem, p_send, p_recv, x_send, x_recv, core_send, core_recv, g_send, g_recv, f_send, f_recv,
-    d_send, d_recv, q_send, q_recv, up_send, down_send, over_send, w_recv,
+    d_send, d_recv, q_send, q_recv, s_send, s_recv, up_send, down_send, over_send, w_recv,
 ):
     me = lax.axis_index("fs")
     tp = lax.axis_index("tp")
@@ -92,8 +95,9 @@
     q, columns = wv_ref.shape
     rows = 2 * q
     rr, rank = fv_ref.shape[0], pv_ref.shape[1]
-    count, early = cut(rows)
-    size = rows // count
+    edges, early = cut(rows)
+    count = len(edges) - 1
+    size = edges[1]
     ways = share(q, t)
     part_rows = q // ways
     streamed = levels <= STREAMED
@@ -174,7 +178,7 @@
 
     def piece(level, side, i):
         column = y if side == 0 else 1 - y
-        return wall.at[level * 2 + column, pl.ds(i * size, size)]
+        return wall.at[level * 2 + column, pl.ds(edges[i], edges[i + 1] - edges[i])]
 
     def along(slot, step):
         side, s, i = line[slot]
@@ -205,6 +209,9 @@
 
     held = set()
 
+    def covering(start, stop):
+        return [i for i in range(count) if edges[i] < stop and edges[i + 1] > start]
+
     def landed(side, level, i):
         place = piece(level, side, i)
         remote(place, place, over_send.at[0], w_recv.at[side, level, i], {"fs": across}).wait_recv()
@@ -233,28 +240,38 @@
     def tight(step):
         return z + step == (levels - 1 if step > 0 else 0)
 
-    def drained(slot):
-        for depth in (DEPTH, DEEP):
-            if 0 <= slot - depth < len(line):
+    done = {"tight": 0, "loose": 0, "over": 0}
+
+    def drained(close, loose):
+        for kind, limit in (("tight", close), ("loose", loose)):
+            for slot in range(done[kind], min(limit, len(line))):
                 for step in (1, -1):
-                    close = tight(step) if depth == DEPTH else jnp.logical_not(tight(step))
-
-                    @pl.when(jnp.logical_and(goes(slot - depth, step), close))
+                    paced = tight(step) if kind == "tight" else jnp.logical_not(tight(step))
+
+                    @pl.when(jnp.logical_and(goes(slot, step), paced))
                     def _():
-                        along(slot - depth, step).wait_send()
-        if slot - DEPTH in over:
-            crossing(slot - DEPTH).wait_send()
+                        along(slot, step).wait_send()
+            done[kind] = max(done[kind], limit)
+        for slot in range(done["over"], close):
+            if slot in over:
+                crossing(slot).wait_send()
+        done["over"] = max(done["over"], close)
 
     def advance(slot):
-        drained(slot)
+        drained(slot - DEPTH + 1, slot - DEEP + 1)
         if slot < len(line):
             side, s, i = line[slot]
             if side == 1 or s > 0:
                 ensure(side, s, i)
             for step in (1, -1):
-                @pl.when(goes(slot, step))
+                @pl.when(jnp.logical_and(goes(slot, step), tight(step)))
                 def _():
                     along(slot, step).start()
+        if 0 <= slot - LATE < len(line):
+            for step in (1, -1):
+                @pl.when(jnp.logical_and(goes(slot - LATE, step), jnp.logical_not(tight(step))))
+                def _():
+                    along(slot - LATE, step).start()
         if slot in over:
             j, i = over[slot]
             for k in range(1, j + 1):
@@ -291,7 +308,7 @@
         if side == 0 and j == 0:
             renew_own(half)
             return
-        for i in range((base[half] + low) // size, -(-(base[half] + high) // size)):
+        for i in covering(base[half] + low, base[half] + high):
             if side == 1 and (i < count - early or j == 0):
                 if i < count - early:
                     crossed(j, i)
@@ -316,7 +333,7 @@
                     fine = 2 * size if j == levels - 1 and q % (2 * size) == 0 else q
                     for low in range(0, q, fine):
                         ready, start = 0, base[half] + low
-                        for i in range(start // size, -(-(start + fine) // size)):
+                        for i in covering(start, start + fine):
                             if side == 1 and (j == 0 or i < count - early):
                                 ready = max(ready, at_over[j, i] + LAG)
                             elif j > 0:
@@ -374,18 +391,27 @@
         )
         pltpu.make_async_copy(x_ref, xin, load_sem.at[3]).wait()
         pr[core] = jnp.dot(xin[...], flat(pall[core]), preferred_element_type=F32).astype(BF16)
-        swapped = go(remote(pr.at[core], pr.at[core], core_send.at[1], core_recv.at[1], {"tp": partner}))
+        chain["swap"] = go(
+            remote(pr.at[core], pr.at[core], core_send.at[1], core_recv.at[1], {"tp": partner})
+        )
+
+    def project(side):
+        grad = lax.dot_general(
+            pr[side], cot[side], (((0,), (0,)), ((), ())), preferred_element_type=F32
+        )
+        for peer in range(n):
+            gsend[peer // 2, peer % 2, :, side * columns:(side + 1) * columns] = (
+                grad[peer * rr:(peer + 1) * rr].astype(BF16)
+            )
+
+    def hook_first():
         for copy in cots:
             copy.wait()
-        swapped.wait_recv()
-        for side in (0, 1):
-            grad = lax.dot_general(
-                pr[side], cot[side], (((0,), (0,)), ((), ())), preferred_element_type=F32
-            )
-            for peer in range(n):
-                gsend[peer // 2, peer % 2, :, side * columns:(side + 1) * columns] = (
-                    grad[peer * rr:(peer + 1) * rr].astype(BF16)
-                )
+        chain["swap"].wait_recv()
+        project(0)
+
+    def hook_second():
+        project(1)
         for d in range(1, levels):
             scatter(d, "start")
         final(ends, gsend.at[z, 1 - y], 0, across, "start")
@@ -473,27 +499,15 @@
             def _():
                 total[...] = gsend[z, y].astype(F32) + fetched(0) + fetched(1) + fetched(2)
 
+        sums = []
         for side, refs in ((0, (nfv, nsv)), (1, (nfo, nso))):
             grad = total[:, side * columns:(side + 1) * columns]
             new_first, new_second, direction = adapt(old[2 * side], old[2 * side + 1], grad)
             refs[0][...] = new_first
             refs[1][...] = new_second
             dall[me, :, side * columns:(side + 1) * columns] = direction
+            sums.append(jnp.sum(jnp.square(direction.astype(F32))))
         chain["dirs"] = spread(lambda block: dall.at[block], d_send, d_recv)
-
-    def hook_dirs():
-        chain["dirs"] = pass_on(chain["dirs"], lambda block: dall.at[block], d_send, d_recv)
-
-    def hook_sums():
-        for copy in chain["dirs"]:
-            copy.wait_recv()
-        sums = []
-        for side in (0, 1):
-            for k in range(n):
-                dir32[k * rr:(k + 1) * rr] = dall[k, :, side * columns:(side + 1) * columns].astype(F32)
-            whole = dir32[...]
-            sums.append(jnp.sum(jnp.square(whole)))
-            dirs[side] = whole.astype(BF16)
         row = lax.broadcasted_iota(jnp.int32, sq.shape[1:], 0)
         sq[tp] = jnp.where(row == 0, sums[0], sums[1])
         chain["sq"] = [
@@ -501,17 +515,34 @@
             for d in range(1, t)
         ]
 
-    def hook_scales():
+    def hook_dirs():
+        chain["dirs"] = pass_on(chain["dirs"], lambda block: dall.at[block], d_send, d_recv)
         for copy in chain["sq"]:
             copy.wait_recv()
+        fsq[me] = jnp.sum(sq[...], axis=0)
+        chain["fsq"] = []
+        for d in range(1, n):
+            target = lax.rem(me + d, n)
+            chain["fsq"].append(go(remote(fsq.at[me], fsq.at[me], s_send.at[d], s_recv.at[d], {"fs": target})))
+
+    def hook_scales():
+        for copy in chain["dirs"]:
+            copy.wait_recv()
+        for side in (0, 1):
+            for k in range(n):
+                dir32[k * rr:(k + 1) * rr] = dall[k, :, side * columns:(side + 1) * columns].astype(F32)
+            dirs[side] = dir32[...].astype(BF16)
+        for copy in chain["fsq"]:
+            copy.wait_recv()
         chain["whole"].wait_recv()
-        totals = jnp.sum(sq[...], axis=0)
+        totals = jnp.sum(fsq[...], axis=0)
         spread_scales = lax.rsqrt(totals / float(rank * columns * t) + norm_eps)
         for side in (0, 1):
             scales[side] = jnp.broadcast_to(spread_scales[side:side + 1], scales.shape[1:])
 
     hooks = dict(zip(HOOKS, (
-        hook_pass, hook_share, hook_grads, hook_partial, hook_moments, hook_dirs, hook_sums, hook_scales
+        hook_pass, hook_share, hook_grads, hook_first, hook_second,
+        hook_partial, hook_moments, hook_dirs, hook_scales,
     )))
     chain["shared"] = []
     chain["proj"] = spread(part, p_send, p_recv)
@@ -519,7 +550,7 @@
         weights[side].wait()
         wall[me, base[side]:base[side] + q] = own[side].astype(BF16)
     units = plan() if streamed else []
-    end = max(slots, max(HOOKS) + 1)
+    end = max(slots, max(HOOKS) + 1, len(line) + LATE)
     for slot in range(end):
         if slot in hooks:
             hooks[slot]()
@@ -531,8 +562,7 @@
                     work(*args)
     for _, _, work, args in units:
         work(*args)
-    for slot in range(end, slots + DEEP):
-        drained(slot)
+    drained(end, end)
 
     for k in range(1, levels):
         for i in range(count):
@@ -592,7 +622,7 @@
     columns = value_cot.shape[1]
     rr = first_value.shape[0]
     levels = n // 2
-    pieces, _ = cut(2 * q)
+    pieces = len(cut(2 * q)[0]) - 1
     ways = share(q, t)
     hbm = pl.BlockSpec(memory_space=pltpu.HBM)
     vmem = pl.BlockSpec(memory_space=pltpu.VMEM)
@@ -630,10 +660,11 @@
             pltpu.VMEM((rank, columns), F32),
             pltpu.VMEM((2, rank, columns), BF16),
             pltpu.VMEM((t, 8, 128), F32),
+            pltpu.VMEM((n, 8, 128), F32),
             pltpu.VMEM((2, 8, 128), F32),
             dma((10,)), dma((n,)), dma((n,)), dma((ways, n)), dma((ways, n)), dma((2,)), dma((2,)),
             dma((levels,)), dma((2, levels)), dma((3,)), dma((3,)), dma((n,)), dma((n,)),
-            dma((t,)), dma((t,)),
+            dma((t,)), dma((t,)), dma((n,)), dma((n,)),
             dma((DEEP,)), dma((DEEP,)), dma((DEPTH,)), dma((2, levels, pieces)),
         ],
         compiler_params=pltpu.CompilerParams(

time: 125 us -> 124 us (level)
  no operation moved by 1% of the time
where the time goes in v4:
time: 124 us; the launch traced here: 123 us
  Pallas kernels  122 us (98%)
    pallas_call x1, Pallas kernels, per_device(): pl.pallas_call(functools.partial(exchange, n, t), out_shape=(pltpu.VMEM((...  117 us
    pallas_call x1, Pallas kernels, per_device(): pl.pallas_call(finish, out_shape=tuple((jax.ShapeDtypeStruct(value.shape,...  4.56 us

profile of v4, /device:TPU:13, one launch (start us, length us, event | category | flops | bytes accessed | tf_op | source)
XLA Modules:
  0.0 122.6 jit_solution(8564501294887044692)
XLA Ops:
  0.6 117.4 %exchange.1 = (bf16[8,288,1024]{2,1,0:T(8,128)(2,1)S(1)}, bf16[1024,2304]{1,0:T(8,128)(2,1)S(1)}, f32[288,1024]{1,0:T(8,128)S(1)}, f32[288,1024]{1,0:T(8,128)S(1...) custom-call(bf16[512,2304]{1,0:T(8,128)(2,1)} %x_ref.1, ...), custom_call_target="tpu_custom_call" | custom-call | tf_op jit(solution)/shard_map/exchange/pallas_call | solution.py:631
  118.1 4.6 %finish.1 = (bf16[2304,1024]{1,0:T(8,128)(2,1)}, bf16[1024,2304]{1,0:T(8,128)(2,1)}, f32[288,1024]{1,0:T(8,128)}, f32[288,1024]{1,0:T(8,128)}, f32[24,1024]{1,0:...) custom-call(bf16[2304,1024]{1,0:T(8,128)(2,1)S(1)} %bitcast.3, ...), custom_call_target="tpu_custom_call" | custom-call | tf_op jit(solution)/shard_map/finish/pallas_call | solution.py:680

commit v5 on v4

--- a/solution.py
+++ b/solution.py
@@ -146,6 +146,9 @@
     cots = [load(vc_ref, cot.at[0], 4), load(ret_ref, cot.at[1], 5)]
     olds = [load(ref, old.at[k], 6 + k) for k, ref in enumerate((fv_ref, sv_ref, fo_ref, so_ref))]
 
+    for side in (0, 1):
+        weights[side].wait()
+        wall[me, base[side]:base[side] + q] = own[side].astype(BF16)
     pltpu.make_async_copy(pv_ref, pall.at[core, me], load_sem.at[0]).wait()
     pl.semaphore_wait(barrier, n - 1 + t - 1)
 
@@ -546,9 +549,6 @@
     )))
     chain["shared"] = []
     chain["proj"] = spread(part, p_send, p_recv)
-    for side in (0, 1):
-        weights[side].wait()
-        wall[me, base[side]:base[side] + q] = own[side].astype(BF16)
     units = plan() if streamed else []
     end = max(slots, max(HOOKS) + 1, len(line) + LATE)
     for slot in range(end):

time: 124 us -> 124 us (level)
  no operation moved by 1% of the time
where the time goes in v5:
time: 124 us; the launch traced here: 123 us
  Pallas kernels  122 us (98%)
    pallas_call x1, Pallas kernels, per_device(): pl.pallas_call(functools.partial(exchange, n, t), out_shape=(pltpu.VMEM((...  117 us
    pallas_call x1, Pallas kernels, per_device(): pl.pallas_call(finish, out_shape=tuple((jax.ShapeDtypeStruct(value.shape,...  4.56 us

profile of v5, /device:TPU:13, one launch (start us, length us, event | category | flops | bytes accessed | tf_op | source)
XLA Modules:
  0.0 122.6 jit_solution(13853680769158119003)
XLA Ops:
  0.6 117.4 %exchange.1 = (bf16[8,288,1024]{2,1,0:T(8,128)(2,1)S(1)}, bf16[1024,2304]{1,0:T(8,128)(2,1)S(1)}, f32[288,1024]{1,0:T(8,128)S(1)}, f32[288,1024]{1,0:T(8,128)S(1...) custom-call(bf16[512,2304]{1,0:T(8,128)(2,1)} %x_ref.1, ...), custom_call_target="tpu_custom_call" | custom-call | tf_op jit(solution)/shard_map/exchange/pallas_call | solution.py:631
  118.1 4.6 %finish.1 = (bf16[2304,1024]{1,0:T(8,128)(2,1)}, bf16[1024,2304]{1,0:T(8,128)(2,1)}, f32[288,1024]{1,0:T(8,128)}, f32[288,1024]{1,0:T(8,128)}, f32[24,1024]{1,0:...) custom-call(bf16[2304,1024]{1,0:T(8,128)(2,1)S(1)} %bitcast.3, ...), custom_call_target="tpu_custom_call" | custom-call | tf_op jit(solution)/shard_map/finish/pallas_call | solution.py:680
